TPU v7x, 128 devices: a whole 4x4x4 slice. The times are simulated.
128 devices in a mesh: sp: 16 (over z, x), tp: 8 (over y, core).
Axes of the slice: x: 4, y: 4, z: 4, core: 2. Of those that a mesh axis runs over, the one named last changes fastest.
Arguments:
- tokens_in: bfloat16 [12288, 2048], P(('sp', 'tp')), may hold values from -300 to 300
- norm_gain: float32 [2048], replicated, may hold values from 0.1 to 1.9
- query_weight: bfloat16 [2048, 1024], P('sp', 'tp'), may hold values from -64 to 64
- key_weight: bfloat16 [2048, 512], P('sp', 'tp'), may hold values from -1 to 1
- value_weight: bfloat16 [2048, 512], P('sp', 'tp'), may hold values from -0.125 to 0.125
- pool_weight: bfloat16 [2048, 1024], P('sp', 'tp'), may hold values from -0.125 to 0.125
- sink_logit: float32 [16], P('tp'), may hold values from 1 to 5
- pool_gain: float32 [1024], P('tp'), may hold values from 0.1 to 1.9
- attention_out_weight: bfloat16 [1024, 2048], P('tp', 'sp'), may hold values from -0.125 to 0.125
- pool_out_weight: bfloat16 [1024, 2048], P('tp', 'sp'), may hold values from -0.1875 to 0.1875
Outputs:
- mixed_out: bfloat16 [12288, 2048], P(('sp', 'tp'))
All inputs are finite; a program needn't handle non-finite values.
Results may differ from a plain program's by a relative error of at most 0.014.
Values may be sent and summed in bfloat16 or wider, within the bound.
A program may use at most 64 MiB of HBM per device.

v0:
```python
import jax
import jax.numpy as jnp
from jax import lax
from jax.sharding import PartitionSpec as P

HEAD_DIM = 64
POOL_CH = 256
POOL_GROUPS = 4
WINDOW = 128


EPS = 1e-06
SHORT_REACHES = (8, 32)


def sent_together(arrays, axis, dim, along):
    ends, at = ([], 0)
    for a in arrays[:-1]:
        at += a.shape[along]
        ends.append(at)
    both = jnp.concatenate(arrays, axis=along)
    return tuple(jnp.split(lax.all_gather(both, axis, axis=dim, tiled=True), ends, axis=along))


def passed_along(block, axis, distance):
    devices = range(lax.axis_size(axis))
    route = [(i - distance, i) for i in devices if i - distance in devices]
    return lax.ppermute(block, axis, route)


def from_everyone(x, axis):
    copies = jnp.broadcast_to(x, (lax.axis_size(axis), *x.shape))
    return lax.all_to_all(copies, axis, split_axis=0, concat_axis=0, tiled=True)


def in_order(parts, dim):
    parts = jnp.moveaxis(parts, 0, dim)
    shape = parts.shape
    return parts.reshape(*shape[:dim], shape[dim] * shape[dim + 1], *shape[dim + 2 :])


def gathered_copies(x, axis, dim):
    parts = from_everyone(x, axis)
    return in_order(parts, dim)


def local(
    tokens_in,
    norm_gain,
    query_weight,
    key_weight,
    value_weight,
    pool_weight,
    sink_logit,
    pool_gain,
    attention_out_weight,
    pool_out_weight,
):
    widened = tokens_in.astype(jnp.float32)
    inverse = lax.rsqrt(jnp.mean(widened * widened, axis=1, keepdims=True) + EPS)
    normed = (widened * inverse * norm_gain).astype(jnp.bfloat16)
    all_rows = lax.all_gather(normed, "tp", axis=0, tiled=True)
    pieces = sent_together((query_weight, key_weight, value_weight, pool_weight), "sp", 0, 1)
    projected = tuple(
        (
            jnp.dot(all_rows, weight_piece, preferred_element_type=jnp.float32)
            for weight_piece in pieces
        )
    )
    query_rows, key_rows, value_rows, pool_rows = [
        projection.astype(jnp.bfloat16) for projection in projected
    ]
    seq_len = query_rows.shape[0]
    offset = lax.axis_index("sp") * seq_len
    halo_keys, halo_values, halo_pool = passed_along(
        (
            key_rows[seq_len - WINDOW :],
            value_rows[seq_len - WINDOW :],
            pool_rows[seq_len - WINDOW :],
        ),
        "sp",
        1,
    )
    kv_local = key_rows.shape[1] // HEAD_DIM
    heads_local = query_rows.shape[1] // HEAD_DIM
    group = heads_local // kv_local
    blocks = seq_len // WINDOW
    key_ext = jnp.concatenate([halo_keys, key_rows], axis=0).reshape(
        blocks + 1, WINDOW, kv_local, HEAD_DIM
    )
    value_ext = jnp.concatenate([halo_values, value_rows], axis=0).reshape(
        blocks + 1, WINDOW, kv_local, HEAD_DIM
    )
    key_pairs = jnp.concatenate([key_ext[:-1], key_ext[1:]], axis=1)
    value_pairs = jnp.concatenate([value_ext[:-1], value_ext[1:]], axis=1)
    query_blocks = query_rows.reshape(blocks, WINDOW, kv_local, group, HEAD_DIM)
    scores = jnp.einsum(
        "nqhgd,nkhd->nhgqk", query_blocks, key_pairs, preferred_element_type=jnp.float32
    ) * HEAD_DIM ** (-0.5)
    shape_mask = (blocks, WINDOW, 2 * WINDOW)
    q_index = lax.broadcasted_iota(jnp.int32, shape_mask, 1)
    k_index = lax.broadcasted_iota(jnp.int32, shape_mask, 2)
    block_index = lax.broadcasted_iota(jnp.int32, shape_mask, 0)
    distance = q_index + WINDOW - k_index
    key_position = offset + block_index * WINDOW + k_index - WINDOW
    allowed = (distance >= 0) & (distance < WINDOW) & (key_position >= 0)
    scores = jnp.where(allowed[:, None, None], scores, -jnp.inf)
    sinks = sink_logit.reshape(1, kv_local, group, 1, 1)
    peak = jnp.maximum(jnp.max(scores, axis=-1, keepdims=True), sinks)
    expo = jnp.exp(scores - peak)
    denom = jnp.sum(expo, axis=-1, keepdims=True) + jnp.exp(sinks - peak)
    probs = (expo / denom).astype(jnp.bfloat16)
    attended = jnp.einsum(
        "nhgqk,nkhd->nqhgd", probs, value_pairs, preferred_element_type=jnp.float32
    )
    attended = attended.astype(jnp.bfloat16).reshape(seq_len, heads_local * HEAD_DIM)
    pool_values = pool_rows.astype(jnp.float32)
    channels = pool_rows.shape[1]
    pool_ext = jnp.concatenate([halo_pool.astype(jnp.float32), pool_values], axis=0)
    running = jnp.concatenate(
        [jnp.zeros((1, channels), jnp.float32), jnp.cumsum(pool_ext, axis=0)], axis=0
    )
    group_id = lax.axis_index("tp") * channels // POOL_CH
    reach = jnp.where(
        group_id == 0, SHORT_REACHES[0], jnp.where(group_id == 1, SHORT_REACHES[1], WINDOW)
    ).astype(jnp.int32)
    upper = running[WINDOW + 1 :]
    lower = lax.dynamic_slice_in_dim(running, WINDOW + 1 - reach, seq_len, 0)
    position = offset + lax.broadcasted_iota(jnp.int32, (seq_len,), 0)
    counted = jnp.minimum(position + 1, reach).astype(jnp.float32)[:, None]
    windowed = (upper - lower) / counted
    own_sums = upper - running[WINDOW]
    device_total = own_sums[seq_len - 1]
    totals = gathered_copies(device_total[None, :], "sp", 0)
    earlier_rows = lax.broadcasted_iota(jnp.int32, (totals.shape[0], 1), 0) < lax.axis_index("sp")
    before = jnp.sum(jnp.where(earlier_rows, totals, 0.0), axis=0)
    cumulative = (before[None, :] + own_sums) / (position + 1).astype(jnp.float32)[:, None]
    pooled = jnp.where(group_id == POOL_GROUPS - 1, cumulative, windowed)
    pool_mixed = ((pooled - pool_values) * pool_gain).astype(jnp.bfloat16)
    out_attend, out_pool = sent_together((attention_out_weight, pool_out_weight), "sp", 1, 0)
    return lax.psum_scatter(
        (
            jnp.dot(attended, out_attend, preferred_element_type=jnp.float32)
            + jnp.dot(pool_mixed, out_pool, preferred_element_type=jnp.float32)
        ).astype(jnp.bfloat16),
        "tp",
        scatter_dimension=0,
        tiled=True,
    )


def solution(mesh):
    in_specs = (
        P(("sp", "tp"), None),
        P(),
        P("sp", "tp"),
        P("sp", "tp"),
        P("sp", "tp"),
        P("sp", "tp"),
        P("tp"),
        P("tp"),
        P("tp", "sp"),
        P("tp", "sp"),
    )
    out_specs = P(("sp", "tp"), None)
    return jax.shard_map(local, mesh=mesh, in_specs=in_specs, out_specs=out_specs, check_vma=False)
```

profile of v0, /device:TPU:0, one launch (start us, length us, event | category | flops | bytes accessed | tf_op | source)
XLA Modules:
  0.0 182.7 jit_solution(4462187103619193170)
XLA Ops:
  6.5 0.8 copy.33
  7.4 0.8 copy.34
  8.2 1.5 pad_maximum_fusion.3
  9.8 1.2 fusion.2
  11.0 1.9 %fusion.4 = bf16[96,2048]{1,0:T(8,128)(2,1)} fusion(bf16[96,2048]{1,0:T(8,128)(2,1)} %param.10, f32[2048]{0:T(1024)} %param.11, f32[96]{0:T(128)S(1)} %add_rsqrt_fusion), kind=kLoop, calls=%fused_computation.15 | loop fusion | flops 786432 | bytes 795008 | tf_op jit(solution)/shard_map/convert_element_type | solution.py:61
  13.8 1.0 fusion.8
  14.7 41.5 %all-gather.6.cloned.1.call-done = bf16[2048,384]{1,0:T(8,128)(2,1)} async-done(((bf16[128,384]{1,0:T(8,128)(2,1)}), bf16[2048,384]{1,0:T(8,128)(2,1)}) %all-gather.6.cloned.1.call-update) | async-done | bytes 1572880 | tf_op jit(solution)/shard_map/all_gather | solution.py:22
  56.2 28.7 %all-gather.4.cloned.1.call-done = bf16[768,2048]{1,0:T(8,128)(2,1)} async-done(((bf16[96,2048]{1,0:T(8,128)(2,1)}), bf16[768,2048]{1,0:T(8,128)(2,1)}) %all-gather.4.cloned.1.call-update) | async-done | bytes 3145744 | tf_op jit(solution)/shard_map/all_gather | solution.py:62
  84.9 3.2 %convolution_convert_fusion.3 = bf16[768,64]{0,1:T(8,128)(2,1)S(1)} fusion(bf16[768,2048]{1,0:T(8,128)(2,1)} %all-gather.4.cloned.1.call-done, bf16[2048,384]{1,0:T(8,128)(2,1)} %all-gather.6.cloned.1.call-done), kind=kOutput, calls=%fused_computation.9 | convolution fusion | flops 201375744 | bytes 3768320 | tf_op jit(solution)/shard_map/dot_general | solution.py:66
  88.9 2.2 %convolution_convert_fusion.4 = bf16[768,64]{0,1:T(8,128)(2,1)S(1)} fusion(bf16[768,2048]{1,0:T(8,128)(2,1)S(1)} %copy-done, bf16[2048,384]{1,0:T(8,128)(2,1)} %all-gather.6.cloned.1.call-done), kind=kOutput, calls=%fused_computation.10 | convolution fusion | flops 201375744 | bytes 3768320 | tf_op jit(solution)/shard_map/dot_general | solution.py:66
  91.9 4.0 %collective-permute-start.1 = (bf16[128,64]{0,1:T(8,128)(2,1)}, bf16[128,64]{0,1:T(8,128)(2,1)}, u32[]{:S(2)}, u32[]{:S(2)}) collective-permute-start(bf16[128,64]{0,1:T(8,128)(2,1)} %slice.62), channel_id=1, source_target_pairs={{0,8},{8,16},{16,24},{24,32},{32,40},{40,48},{48,56},{56,64},{64,7... | collective-permute-start | bytes 49160 | tf_op jit(solution)/shard_map/ppermute | solution.py:28
  96.5 3.4 %collective-permute-start = (bf16[128,64]{0,1:T(8,128)(2,1)}, bf16[128,64]{0,1:T(8,128)(2,1)}, u32[]{:S(2)}, u32[]{:S(2)}) collective-permute-start(bf16[128,64]{0,1:T(8,128)(2,1)} %slice.61), channel_id=1, source_target_pairs={{0,8},{8,16},{16,24},{24,32},{32,40},{40,48},{48,56},{56,64},{64,7... | collective-permute-start | bytes 49160 | tf_op jit(solution)/shard_map/ppermute | solution.py:28
  100.6 2.0 %fusion.45 = (f32[768,128]{1,0:T(8,128)S(1)}, bf16[768,128]{1,0:T(8,128)(2,1)S(1)}) fusion(bf16[768,2048]{1,0:T(8,128)(2,1)S(1)} %copy-done, bf16[2048,384]{1,0:T(8,128)(2,1)} %all-gather.6.cloned.1.call-done), kind=kOutput, calls=%fused_computation.79 | convolution fusion | flops 402849792 | bytes 4259840 | tf_op jit(solution)/shard_map/dot_general | solution.py:66
  103.8 3.1 %collective-permute-start.2 = (bf16[128,128]{1,0:T(8,128)(2,1)}, bf16[128,128]{1,0:T(8,128)(2,1)}, u32[]{:S(2)}, u32[]{:S(2)}) collective-permute-start(bf16[128,128]{1,0:T(8,128)(2,1)} %slice.63), channel_id=1, source_target_pairs={{0,8},{8,16},{16,24},{24,32},{32,40},{40,48},{48,56},{56,64},{64,7... | collective-permute-start | bytes 98312 | tf_op jit(solution)/shard_map/ppermute | solution.py:28
  106.9 2.7 %convolution_convert_fusion.1 = bf16[768,128]{1,0:T(8,128)(2,1)} fusion(bf16[768,2048]{1,0:T(8,128)(2,1)S(1)} %copy-done, bf16[2048,384]{1,0:T(8,128)(2,1)} %all-gather.6.cloned.1.call-done), kind=kOutput, calls=%fused_computation.6 | convolution fusion | flops 402751488 | bytes 3866624 | tf_op jit(solution)/shard_map/dot_general | solution.py:66
  109.6 1.1 reshape.121
  110.8 0.9 pad_maximum_fusion.1
  111.8 1.5 fusion.44
  115.2 0.8 convert_element_type.66
  117.1 6.1 %all-to-all-start = ((f32[16,1,128]{2,1,0:T(1,128)}), f32[16,1,128]{2,1,0:T(1,128)S(1)}, u32[]{:S(2)}, u32[]{:S(2)}) async-start(f32[16,1,128]{2,1,0:T(1,128)} %broadcast_in_dim.40), calls=%async_computation | async-start | bytes 16384 | tf_op jit(solution)/shard_map/all_to_all | solution.py:33
  123.3 7.0 %all-gather.8.cloned.1.call-done = bf16[256,2048]{1,0:T(8,128)(2,1)} async-done(((bf16[256,128]{1,0:T(8,128)(2,1)}), bf16[256,2048]{1,0:T(8,128)(2,1)}) %all-gather.8.cloned.1.call-update) | async-done | bytes 1048592 | tf_op jit(solution)/shard_map/all_gather | solution.py:22
  130.3 4.8 %fusion.12 = f32[768,2048]{1,0:T(8,128)} fusion(bf16[256,2048]{1,0:T(8,128)(2,1)} %all-gather.8.cloned.1.call-done, bf16[16,8,6,128]{3,2,1,0:T(8,128)(2,1)S(1)} %bitcast.62), kind=kOutput, calls=%fused_computation.25 | convolution fusion | flops 402653184 | bytes 7012352 | tf_op jit(solution)/shard_map/dot_general | solution.py:143
  135.2 5.6 %add_convert_fusion = bf16[768,2048]{1,0:T(8,128)(2,1)} fusion(f32[768,2048]{1,0:T(8,128)} %fusion.12, bf16[256,2048]{1,0:T(8,128)(2,1)S(1)} %copy-done.3, s32[]{:T(128)S(6)} %select_n.38, f32[896,128]{1,0:T(8,128)S(1)} %bitcast.60, f32[768,128]{1,0:T(8,128)S(1)} %slice_subtract_fusion, f32[128]{0:T(128)S(1)} %copy-done.11, f32[768]{0:T(1024)S(1)} %get-tuple-element.9, ...), kind=kOutput, calls=%fused_computation | convolution fusion | flops 406683648 | bytes 11412485 | tf_op jit(solution)/shard_map/dot_general | solution.py:144
  140.8 35.3 %reduce-scatter.2.cloned.1.call-done = bf16[96,2048]{1,0:T(8,128)(2,1)} async-done(((bf16[768,2048]{1,0:T(8,128)(2,1)}), bf16[96,2048]{1,0:T(8,128)(2,1)}) %reduce-scatter.2.cloned.1.call-update) | async-done | bytes 393232 | tf_op jit(solution)/shard_map/reduce_scatter | solution.py:141
  (70 shorter events, 8.2 us)
Async XLA Ops:
  6.5 6.4 %copy-start.8 = (bf16[128,128]{1,0:T(8,128)(2,1)S(1)}, bf16[128,128]{1,0:T(8,128)(2,1)}, u32[]{:S(2)}) copy-start(bf16[128,128]{1,0:T(8,128)(2,1)} %param.19) | copy-start | bytes 98308
  6.5 6.5 %copy-start.9 = (bf16[128,128]{1,0:T(8,128)(2,1)S(1)}, bf16[128,128]{1,0:T(8,128)(2,1)}, u32[]{:S(2)}) copy-start(bf16[128,128]{1,0:T(8,128)(2,1)} %param.18) | copy-start | bytes 98308
  6.5 49.7 %all-gather.6.cloned.1.call-start = ((), (), s32[]{:S(2)}) async-start(), calls=%async_computation.3 | async-start | bytes 1671168 | tf_op jit(solution)/shard_map/all_gather | solution.py:22
  9.7 75.1 %all-gather.4.cloned.1.call-start = ((), (), s32[]{:S(2)}) async-start(), calls=%async_computation.2 | async-start | bytes 3538944 | tf_op jit(solution)/shard_map/all_gather | solution.py:62
  12.9 117.4 %all-gather.8.cloned.1.call-start = ((), (), s32[]{:S(2)}) async-start(), calls=%async_computation.4 | async-start | bytes 1114112 | tf_op jit(solution)/shard_map/all_gather | solution.py:22
  84.9 4.0 %copy-start = (bf16[768,2048]{1,0:T(8,128)(2,1)S(1)}, bf16[768,2048]{1,0:T(8,128)(2,1)}, u32[]{:S(2)}) copy-start(bf16[768,2048]{1,0:T(8,128)(2,1)} %all-gather.4.cloned.1.call-done) | copy-start | bytes 9437188
  88.1 0.7 copy-start.6
  91.1 8.8 %copy-start.4 = (bf16[768,64]{0,1:T(8,128)(2,1)}, bf16[768,64]{0,1:T(8,128)(2,1)S(1)}, u32[]{:S(2)}) copy-start(bf16[768,64]{0,1:T(8,128)(2,1)S(1)} %convolution_convert_fusion.4) | copy-start | bytes 294916
  91.9 18.8 %collective-permute-start.1 = (bf16[128,64]{0,1:T(8,128)(2,1)}, bf16[128,64]{0,1:T(8,128)(2,1)}, u32[]{:S(2)}, u32[]{:S(2)}) collective-permute-start(bf16[128,64]{0,1:T(8,128)(2,1)} %slice.62), channel_id=1, source_target_pairs={{0,8},{8,16},{16,24},{24,32},{32,40},{40,48},{48,56},{56,64},{64,7... | collective-permute-start | bytes 49160 | tf_op jit(solution)/shard_map/ppermute | solution.py:28
  96.5 17.2 %collective-permute-start = (bf16[128,64]{0,1:T(8,128)(2,1)}, bf16[128,64]{0,1:T(8,128)(2,1)}, u32[]{:S(2)}, u32[]{:S(2)}) collective-permute-start(bf16[128,64]{0,1:T(8,128)(2,1)} %slice.61), channel_id=1, source_target_pairs={{0,8},{8,16},{16,24},{24,32},{32,40},{40,48},{48,56},{56,64},{64,7... | collective-permute-start | bytes 49160 | tf_op jit(solution)/shard_map/ppermute | solution.py:28
  102.6 0.7 copy-start.1
  103.8 11.4 %collective-permute-start.2 = (bf16[128,128]{1,0:T(8,128)(2,1)}, bf16[128,128]{1,0:T(8,128)(2,1)}, u32[]{:S(2)}, u32[]{:S(2)}) collective-permute-start(bf16[128,128]{1,0:T(8,128)(2,1)} %slice.63), channel_id=1, source_target_pairs={{0,8},{8,16},{16,24},{24,32},{32,40},{40,48},{48,56},{56,64},{64,7... | collective-permute-start | bytes 98312 | tf_op jit(solution)/shard_map/ppermute | solution.py:28
  111.7 1.7 copy-start.10
  111.8 1.9 %copy-start.5 = (bf16[768,64]{0,1:T(8,128)(2,1)S(1)}, bf16[768,64]{0,1:T(8,128)(2,1)}, u32[]{:S(2)}) copy-start(bf16[768,64]{0,1:T(8,128)(2,1)} %copy-done.4) | copy-start | bytes 294916
  113.3 1.3 copy-start.7
  117.1 18.0 %all-to-all-start = ((f32[16,1,128]{2,1,0:T(1,128)}), f32[16,1,128]{2,1,0:T(1,128)S(1)}, u32[]{:S(2)}, u32[]{:S(2)}) async-start(f32[16,1,128]{2,1,0:T(1,128)} %broadcast_in_dim.40), calls=%async_computation | async-start | bytes 16384 | tf_op jit(solution)/shard_map/all_to_all | solution.py:33
  123.3 52.8 %reduce-scatter.2.cloned.1.call-start = ((), (), s32[]{:S(2)}) async-start(), calls=%async_computation.5 | async-start | bytes 3538944 | tf_op jit(solution)/shard_map/reduce_scatter | solution.py:141
  130.3 4.9 %copy-start.2 = (bf16[768,128]{1,0:T(8,128)(2,1)S(1)}, bf16[768,128]{1,0:T(8,128)(2,1)}, u32[]{:S(2)}) copy-start(bf16[768,128]{1,0:T(8,128)(2,1)} %copy-done.1) | copy-start | bytes 589828
  130.3 4.9 %copy-start.3 = (bf16[256,2048]{1,0:T(8,128)(2,1)S(1)}, bf16[256,2048]{1,0:T(8,128)(2,1)}, u32[]{:S(2)}) copy-start(bf16[256,2048]{1,0:T(8,128)(2,1)} %all-gather.8.cloned.1.call-done) | copy-start | bytes 3145732
  130.3 4.9 %copy-start.11 = (f32[128]{0:T(128)S(1)}, f32[128]{0:T(128)}, u32[]{:S(2)}) copy-start(f32[128]{0:T(128)} %param.17) | copy-start | bytes 1540
Sparse Core Ops, SparseCore 0:
  9.9 46.2 all-gather.5
  57.9 26.9 all-gather.3
  87.0 43.2 all-gather.7
  141.0 35.1 reduce-scatter.1
where the time goes:
time: 183 us
  waiting for transfers between devices  112 us (61%)
  matrix products  22.4 us (12%)
  starting transfers between devices  16.7 us (9%)
  between operations  13.5 us (7%)
  other arithmetic  9.51 us (5%)
  local copies, waits for them, and re-layouts  8.08 us (4%)
    all_gather x2, waiting for transfers between devices, sent_together(): lax.all_gather(both, axis, axis=dim, tiled=True)  48.4 us
    reduce_scatter x1, waiting for transfers between devices, local(): lax.psum_scatter((jnp.dot(attended, out_attend, preferred_element_type=jn...  35.3 us
    all_gather x1, waiting for transfers between devices, local(): all_rows = lax.all_gather(normed, 'tp', axis=0, tiled=True)  28.7 us
    ppermute x3, starting transfers between devices, passed_along(): return lax.ppermute(block, axis, route)  10.4 us
    dot_general x4, matrix products, local(): jnp.dot(all_rows, weight_piece, preferred_element_type=jnp.float32)  10.1 us
    all_to_all x1, starting transfers between devices, from_everyone(): return lax.all_to_all(copies, axis, split_axis=0, concat_axis=0, tiled=True)  6.14 us
    dot_general x1, matrix products, local(): jnp.dot(pool_mixed, out_pool, preferred_element_type=jnp.float32)  5.6 us
    dot_general x1, matrix products, local(): jnp.dot(attended, out_attend, preferred_element_type=jnp.float32)  4.8 us
  transfers between devices with their start and end apart: 8, of which 4 were waited for; matrix products, arithmetic and copies ran while one was open for 17% of the time, Pallas kernels for 0%

commit v1 on v0

v1 whole, which is shorter than its diff:
```python
import jax
import jax.numpy as jnp
from jax import lax
from jax.experimental import pallas as pl
from jax.experimental.pallas import tpu as pltpu
from jax.sharding import PartitionSpec as P

MESH = pl.DeviceIdType.MESH
F32 = jnp.float32
BF16 = jnp.bfloat16

D = 2048
HEAD_DIM = 64
WINDOW = 128
EPS = 1e-06
SIDE = 4
PLANE = SIDE * SIDE
BLOCK = 96
HALF = BLOCK // 2
ROWS = 2 * SIDE * BLOCK
CHUNK = 2 * BLOCK
DEPTH = D // PLANE
IN_COLS = 384
N_MSG = 144


class Messages:
    def __init__(self, send_sems, recv_sems):
        self.send_sems, self.recv_sems, self.made = send_sems, recv_sems, []

    def new(self, src, dst, device, land):
        number = len(self.made)
        message = Message(
            lambda a, b: pltpu.make_async_remote_copy(
                src_ref=a,
                dst_ref=b,
                send_sem=self.send_sems.at[number],
                recv_sem=self.recv_sems.at[number],
                device_id=device,
                device_id_type=MESH,
            ),
            src,
            dst,
            land,
        )
        self.made.append(message)
        return message


class Message:
    def __init__(self, make, src, dst, land):
        self.make, self.src, self.dst, self.land = make, src, dst, land

    def start(self):
        self.make(self.src, self.dst).start()

    def arrived(self):
        self.make(self.land, self.land).wait_recv()

    def sent(self):
        self.make(self.src, self.dst).wait_send()


def rows_of(start, size, unit=16):
    return pl.ds(pl.multiple_of(start, unit), size)


def kernel(
    x_hbm,
    gain_hbm,
    wq_hbm,
    wk_hbm,
    wv_hbm,
    wp_hbm,
    sink_ref,
    pgain_hbm,
    wa_hbm,
    wo_hbm,
    out_ref,
    xin,
    gain,
    pgain,
    wk,
    wv,
    tok,
    win,
    wout,
    qbuf,
    kvsend,
    kvland,
    kp0,
    kp1,
    vp0,
    vp1,
    pext,
    tot,
    tots,
    sraw,
    amine,
    apart,
    far,
    nbn,
    nbp,
    accn,
    accp,
    rfn,
    rfp,
    rn,
    rp,
    local_sems,
    send_sems,
    recv_sems,
):
    sp = lax.axis_index("sp")
    tp = lax.axis_index("tp")
    z, x = sp // SIDE, lax.rem(sp, SIDE)
    y, c = tp // 2, lax.rem(tp, 2)
    other = 1 - c

    def turn(i, by):
        return lax.rem(i + by + SIDE, SIDE)

    yn, yp, yf = turn(y, 1), turn(y, -1), turn(y, 2)
    partner = (sp, y * 2 + other)
    up, down = (sp, yn * 2 + c), (sp, yp * 2 + c)

    own_in = rows_of(sp * DEPTH, DEPTH, 128)
    own_cols = rows_of(sp * 128, 128, 128)
    loads = [
        (x_hbm, xin),
        (gain_hbm, gain),
        (wk_hbm, wk),
        (wv_hbm, wv),
        (wq_hbm, win.at[own_in, pl.ds(0, 128)]),
        (wp_hbm, win.at[own_in, pl.ds(256, 128)]),
        (pgain_hbm, pgain),
        (wa_hbm, wout.at[pl.ds(0, 128), own_cols]),
        (wo_hbm, wout.at[pl.ds(128, 128), own_cols]),
    ]
    loads = [pltpu.make_async_copy(a, b, local_sems.at[n]) for n, (a, b) in enumerate(loads)]
    for load in loads:
        load.start()

    barrier = pltpu.get_barrier_semaphore()
    for step in range(1, PLANE):
        peer = (lax.rem(sp + step, PLANE), tp)
        pl.semaphore_signal(barrier, inc=1, device_id=peer, device_id_type=MESH)
    for peer in (up, down, partner):
        pl.semaphore_signal(barrier, inc=1, device_id=peer, device_id_type=MESH)

    loads[0].wait()
    loads[1].wait()
    gains = gain[...]
    for r in range(0, BLOCK, 16):
        wide = xin[pl.ds(r, 16)].astype(F32)
        inverse = lax.rsqrt(jnp.mean(wide * wide, axis=1, keepdims=True) + EPS)
        tok[rows_of(tp * BLOCK + r, 16), :] = (wide * inverse * gains).astype(BF16)
    loads[2].wait()
    loads[3].wait()
    win[own_in, pl.ds(128, 128)] = jnp.concatenate([wk[...], wv[...]], axis=1)
    for load in loads[4:]:
        load.wait()

    messages = Messages(send_sems, recv_sems)

    def block(yy, cc):
        return tok.at[rows_of((yy * 2 + cc) * BLOCK, BLOCK)]

    def half(yy, cc, h):
        return tok.at[rows_of((yy * 2 + cc) * BLOCK + h * HALF, HALF)]

    t_n0 = messages.new(half(y, c, 0), half(y, c, 0), up, half(yp, c, 0))
    t_p1 = messages.new(half(y, c, 1), half(y, c, 1), down, half(yn, c, 1))
    t_n1 = messages.new(half(y, c, 1), half(y, c, 1), up, half(yp, c, 1))
    t_p0 = messages.new(half(y, c, 0), half(y, c, 0), down, half(yn, c, 0))
    f_n = messages.new(half(yp, c, 0), half(yp, c, 0), up, half(yf, c, 0))
    f_p = messages.new(half(yn, c, 1), half(yn, c, 1), down, half(yf, c, 1))
    d_own = messages.new(block(y, c), block(y, c), partner, block(y, other))

    def across(yy, h):
        return messages.new(half(yy, c, h), half(yy, c, h), partner, half(yy, other, h))

    d_p0, d_n1, d_p1, d_n0 = across(yp, 0), across(yn, 1), across(yp, 1), across(yn, 0)
    d_f0, d_f1 = across(yf, 0), across(yf, 1)

    class Gather:
        def __init__(self, group, piece, sub):
            def source(o1, o2):
                if group == 0:
                    return turn(z, o2) * SIDE + turn(x, o1)
                return turn(z, o1) * SIDE + turn(x, o2)

            def device(o1, o2):
                return (source(o1, o2), tp)

            def send(ref, o1, o2, land):
                return messages.new(ref, ref, device(o1, o2), land)

            s = source
            self.a_n = send(piece(s(0, 0)), 1, 0, piece(s(-1, 0)))
            self.a_p = send(piece(s(0, 0)), -1, 0, piece(s(1, 0)))
            self.a_fn = send(sub(s(-1, 0), 0), 1, 0, sub(s(2, 0), 0))
            self.a_fp = send(sub(s(1, 0), 1), -1, 0, sub(s(2, 0), 1))
            self.b_n, self.b_p, self.b_fn, self.b_fp = {}, {}, {}, {}
            for o in (0, -1, 1, 2):
                self.b_n[o] = send(piece(s(o, 0)), 0, 1, piece(s(o, -1)))
                self.b_p[o] = send(piece(s(o, 0)), 0, -1, piece(s(o, 1)))
                self.b_fn[o] = send(sub(s(o, -1), 0), 0, 1, sub(s(o, 2), 0))
                self.b_fp[o] = send(sub(s(o, 1), 1), 0, -1, sub(s(o, 2), 1))

        def begin(self):
            self.a_n.start()
            self.a_p.start()
            self.cross(0)

        def cross(self, o):
            self.b_n[o].start()
            self.b_p[o].start()

        def near(self):
            self.a_n.arrived()
            self.a_fn.start()
            self.a_p.arrived()
            self.a_fp.start()
            self.cross(-1)
            self.cross(1)

        def distant(self):
            self.a_fn.arrived()
            self.a_fp.arrived()
            self.cross(2)

        def pass_on(self, o):
            self.b_n[o].arrived()
            self.b_fn[o].start()
            self.b_p[o].arrived()
            self.b_fp[o].start()

        def finish(self):
            for o in (0, -1, 1, 2):
                self.b_fn[o].arrived()
                self.b_fp[o].arrived()

    def in_piece(group):
        size = DEPTH // 2
        return (
            lambda s: win.at[rows_of(s * DEPTH + group * size, size)],
            lambda s, h: win.at[rows_of(s * DEPTH + group * size + h * (size // 2), size // 2)],
        )

    def out_piece(group):
        return (
            lambda s: wout.at[pl.ds(group * 128, 128), rows_of(s * 128, 128, 128)],
            lambda s, h: wout.at[pl.ds(group * 128 + h * 64, 64), rows_of(s * 128, 128, 128)],
        )

    ins = [Gather(g, *in_piece(g)) for g in range(2)]
    outs = [Gather(g, *out_piece(g)) for g in range(2)]
    d_out = messages.new(
        wout.at[pl.ds(0, 256)], wout.at[pl.ds(256, 256)], partner, wout.at[pl.ds(256, 256)]
    )

    pl.semaphore_wait(barrier, PLANE - 1 + 3)

    for m in (t_n0, t_p1, t_n1, t_p0):
        m.start()
    for g in ins:
        g.begin()
    d_own.start()
    for g in ins:
        g.near()
    for g in ins:
        g.pass_on(0)
    for g in ins:
        g.distant()
    t_n0.arrived()
    f_n.start()
    d_p0.start()
    t_p1.arrived()
    f_p.start()
    d_n1.start()
    for g in ins:
        g.pass_on(-1)
        g.pass_on(1)
    for g in ins:
        g.pass_on(2)
    for g in outs:
        g.begin()
    for g in outs:
        g.near()
    for g in outs:
        g.pass_on(0)
    for g in outs:
        g.distant()
    for g in ins:
        g.finish()
    t_n1.arrived()
    d_p1.start()
    t_p0.arrived()
    d_n0.start()

    lane = lax.broadcasted_iota(jnp.int32, (CHUNK, 128), 1)

    def spread(kv, rows, at):
        first = lax.broadcasted_iota(jnp.int32, (rows, 128), 1) < HEAD_DIM
        turned = pltpu.roll(kv, HEAD_DIM, 1)
        kp0[at, :] = jnp.where(first, kv, 0.0).astype(BF16)
        kp1[at, :] = jnp.where(first, 0.0, turned).astype(BF16)
        vp0[at, :] = jnp.where(first, turned, 0.0).astype(BF16)
        vp1[at, :] = jnp.where(first, 0.0, kv).astype(BF16)

    def project(yy):
        at = rows_of(yy * CHUNK, CHUNK)
        got = jnp.dot(tok[at, :], win[...], preferred_element_type=F32)
        qbuf[at, :] = got[:, :128].astype(BF16)
        ahead = rows_of(yy * CHUNK + WINDOW, CHUNK)
        spread(got[:, 128:256].astype(BF16).astype(F32), CHUNK, ahead)
        pool = got[:, 256:].astype(BF16)
        pext[ahead, :] = pool
        return jnp.sum(pool.astype(F32).reshape(CHUNK // 8, 8, 128), axis=0)

    d_own.arrived()
    total = project(y)
    for g in outs:
        g.pass_on(-1)
        g.pass_on(1)
    d_p0.arrived()
    d_p1.arrived()
    total = total + project(yp)
    for g in outs:
        g.pass_on(2)
    d_n0.arrived()
    d_n1.arrived()
    total = total + project(yn)
    for g in outs:
        g.finish()
    d_out.start()
    f_n.arrived()
    d_f0.start()
    f_p.arrived()
    d_f1.start()
    d_f0.arrived()
    d_f1.arrived()
    total = total + project(yf)

    last = pl.ds(ROWS, WINDOW)
    kvsend[...] = kp0[last, :] + vp1[last, :]
    after = (lax.rem(sp + 1, PLANE), tp)
    h_kv = messages.new(kvsend, kvland, after, kvland)
    h_p = messages.new(pext.at[last], pext.at[pl.ds(0, WINDOW)], after, pext.at[pl.ds(0, WINDOW)])
    h_kv.start()
    h_p.start()
    tot[...] = total
    sums = []
    for step in range(1, PLANE):
        m = messages.new(
            tot,
            tots.at[sp],
            (lax.rem(sp + step, PLANE), tp),
            tots.at[lax.rem(sp + PLANE - step, PLANE)],
        )
        m.start()
        sums.append(m)
    tots[sp] = total

    q_index = lax.broadcasted_iota(jnp.int32, (WINDOW, 2 * WINDOW), 0)
    k_index = lax.broadcasted_iota(jnp.int32, (WINDOW, 2 * WINDOW), 1)
    distance = q_index + WINDOW - k_index
    reach = jnp.where(y == 0, 8, jnp.where(y == 1, 32, jnp.where(y == 2, WINDOW, 1 << 24)))
    inside = (distance >= 0) & (distance < WINDOW)
    banded = (distance >= 0) & (distance < reach) & ((k_index >= WINDOW) | (y < 3))
    sinks = (sink_ref[0], sink_ref[1])

    def probabilities(q, keys, allowed, sink):
        scores = lax.dot_general(q, keys, (((1,), (1,)), ((), ())), preferred_element_type=F32)
        scores = jnp.where(allowed, scores * HEAD_DIM ** (-0.5), -jnp.inf)
        peak = jnp.maximum(jnp.max(scores, axis=1, keepdims=True), sink)
        expo = jnp.exp(scores - peak)
        denom = jnp.sum(expo, axis=1, keepdims=True) + jnp.exp(sink - peak)
        return (expo * (1.0 / denom)).astype(BF16)

    def attend(b):
        at, pair = pl.ds(b * WINDOW, WINDOW), pl.ds(b * WINDOW, 2 * WINDOW)
        allowed, band = inside, banded
        if b == 0:
            present = (k_index >= WINDOW) | (sp > 0)
            allowed, band = allowed & present, band & present
        q = qbuf[at, :]
        p0 = probabilities(q, kp0[pair, :], allowed, sinks[0])
        p1 = probabilities(q, kp1[pair, :], allowed, sinks[1])
        mixed = jnp.dot(p0, vp0[pair, :], preferred_element_type=F32)
        mixed = mixed + jnp.dot(p1, vp1[pair, :], preferred_element_type=F32)
        amine[at, pl.ds(0, 128)] = mixed.astype(BF16)
        ones = jnp.where(band, 1.0, 0.0).astype(BF16)
        sraw[at, :] = jnp.dot(ones, pext[pair, :], preferred_element_type=F32)

    for b in range(1, ROWS // WINDOW):
        attend(b)
    h_kv.arrived()
    h_p.arrived()
    spread(kvland[...].astype(F32), WINDOW, pl.ds(0, WINDOW))
    attend(0)

    for m in sums:
        m.arrived()
    earlier = lax.broadcasted_iota(jnp.int32, (PLANE, 8, 128), 0) < sp
    before = jnp.sum(jnp.sum(jnp.where(earlier, tots[...], 0.0), axis=0), axis=0, keepdims=True)
    carry = jnp.where(y == 3, before, 0.0)
    pool_gain = pgain[...]
    for b in range(ROWS // WINDOW):
        at = pl.ds(b * WINDOW, WINDOW)
        position = sp * ROWS + b * WINDOW + lax.broadcasted_iota(jnp.int32, (WINDOW, 128), 0)
        count = jnp.minimum(position + 1, reach).astype(F32)
        here = sraw[at, :]
        value = pext[pl.ds((b + 1) * WINDOW, WINDOW), :].astype(F32)
        amine[at, pl.ds(128, 128)] = (((here + carry) / count - value) * pool_gain).astype(BF16)
        carry = carry + jnp.where(y == 3, here[WINDOW - 1 :, :], 0.0)

    swaps = []
    for yy in (yf, yn, yp, y):
        src = amine.at[rows_of((yy * 2 + other) * BLOCK, BLOCK)]
        dst = apart.at[rows_of(yy * BLOCK, BLOCK)]
        m = messages.new(src, dst, partner, dst)
        m.start()
        swaps.append(m)
    d_out.arrived()

    def product(yy, put):
        mine = amine[rows_of((yy * 2 + c) * BLOCK, BLOCK), :]
        theirs = apart[rows_of(yy * BLOCK, BLOCK), :]
        for n in range(0, D, 512):
            cols = pl.ds(n, 512)
            got = jnp.dot(mine, wout[pl.ds(0, 256), cols], preferred_element_type=F32)
            got = got + jnp.dot(theirs, wout[pl.ds(256, 256), cols], preferred_element_type=F32)
            put(cols, got)

    top, bottom = pl.ds(0, HALF), pl.ds(HALF, HALF)
    r_fn = messages.new(far.at[top], rfn, up, rfn)
    r_fp = messages.new(far.at[bottom], rfp, down, rfp)
    r_n1 = messages.new(nbn.at[bottom], rn.at[bottom], up, rn.at[bottom])
    r_p0 = messages.new(nbp.at[top], rp.at[top], down, rp.at[top])
    r_n0 = messages.new(nbn.at[top], rn.at[top], up, rn.at[top])
    r_p1 = messages.new(nbp.at[bottom], rp.at[bottom], down, rp.at[bottom])

    def put_far(cols, got):
        far[:, cols] = got.astype(BF16)

    def put_next(cols, got):
        nbn[bottom, cols] = got[HALF:].astype(BF16)
        accn[:, cols] = got[:HALF]

    def put_prev(cols, got):
        nbp[top, cols] = got[:HALF].astype(BF16)
        accp[:, cols] = got[HALF:]

    swaps[0].arrived()
    product(yf, put_far)
    r_fn.start()
    r_fp.start()
    swaps[1].arrived()
    product(yn, put_next)
    r_n1.start()
    swaps[2].arrived()
    product(yp, put_prev)
    r_p0.start()
    r_fn.arrived()
    nbn[top, :] = (accn[...] + rfn[...].astype(F32)).astype(BF16)
    r_n0.start()
    r_fp.arrived()
    nbp[bottom, :] = (accp[...] + rfp[...].astype(F32)).astype(BF16)
    r_p1.start()

    swaps[3].arrived()

    def put_own(cols, got):
        accn[:, cols] = got[:HALF]
        accp[:, cols] = got[HALF:]

    product(y, put_own)
    r_n1.arrived()
    accp[...] = accp[...] + rn[bottom, :].astype(F32)
    r_p0.arrived()
    accn[...] = accn[...] + rp[top, :].astype(F32)
    r_n0.arrived()
    out_ref[top, :] = (accn[...] + rn[top, :].astype(F32)).astype(BF16)
    r_p1.arrived()
    out_ref[bottom, :] = (accp[...] + rp[bottom, :].astype(F32)).astype(BF16)
    for m in messages.made:
        m.sent()
    assert len(messages.made) <= N_MSG


def local(
    tokens_in,
    norm_gain,
    query_weight,
    key_weight,
    value_weight,
    pool_weight,
    sink_logit,
    pool_gain,
    attention_out_weight,
    pool_out_weight,
):
    hbm = pl.BlockSpec(memory_space=pl.ANY)
    scratch = [
        ((BLOCK, D), BF16),
        ((1, D), F32),
        ((1, 128), F32),
        ((DEPTH, 64), BF16),
        ((DEPTH, 64), BF16),
        ((ROWS, D), BF16),
        ((D, IN_COLS), BF16),
        ((512, D), BF16),
        ((ROWS, 128), BF16),
        ((WINDOW, 128), BF16),
        ((WINDOW, 128), BF16),
        ((ROWS + WINDOW, 128), BF16),
        ((ROWS + WINDOW, 128), BF16),
        ((ROWS + WINDOW, 128), BF16),
        ((ROWS + WINDOW, 128), BF16),
        ((ROWS + WINDOW, 128), BF16),
        ((8, 128), F32),
        ((PLANE, 8, 128), F32),
        ((ROWS, 128), F32),
        ((ROWS, 256), BF16),
        ((SIDE * BLOCK, 256), BF16),
        ((BLOCK, D), BF16),
        ((BLOCK, D), BF16),
        ((BLOCK, D), BF16),
        ((HALF, D), F32),
        ((HALF, D), F32),
        ((HALF, D), BF16),
        ((HALF, D), BF16),
        ((BLOCK, D), BF16),
        ((BLOCK, D), BF16),
    ]
    return pl.pallas_call(
        kernel,
        out_shape=jax.ShapeDtypeStruct((BLOCK, D), BF16),
        in_specs=[hbm] * 6 + [pl.BlockSpec(memory_space=pltpu.SMEM)] + [hbm] * 3,
        out_specs=pl.BlockSpec(memory_space=pltpu.VMEM),
        scratch_shapes=[pltpu.VMEM(shape, kind) for shape, kind in scratch]
        + [
            pltpu.SemaphoreType.DMA((9,)),
            pltpu.SemaphoreType.DMA((N_MSG,)),
            pltpu.SemaphoreType.DMA((N_MSG,)),
        ],
        compiler_params=pltpu.CompilerParams(
            collective_id=0, has_side_effects=True, vmem_limit_bytes=40 * 1024 * 1024
        ),
    )(
        tokens_in,
        norm_gain.reshape(1, D),
        query_weight,
        key_weight,
        value_weight,
        pool_weight,
        sink_logit,
        pool_gain.reshape(1, 128),
        attention_out_weight,
        pool_out_weight,
    )


def solution(mesh):
    in_specs = (
        P(("sp", "tp"), None),
        P(),
        P("sp", "tp"),
        P("sp", "tp"),
        P("sp", "tp"),
        P("sp", "tp"),
        P("tp"),
        P("tp"),
        P("tp", "sp"),
        P("tp", "sp"),
    )
    out_specs = P(("sp", "tp"), None)
    return jax.shard_map(local, mesh=mesh, in_specs=in_specs, out_specs=out_specs, check_vma=False)
```

time: 183 us -> 68.9 us (0.38)
  waiting for transfers between devices: 112 us -> 0 us
  Pallas kernels: 0 us -> 63.6 us
  matrix products: 22.4 us -> 0 us
  starting transfers between devices: 16.7 us -> 0 us
  between operations: 13.5 us -> 0.07 us
  other arithmetic: 9.51 us -> 0 us
  local copies, waits for them, and re-layouts: 8.08 us -> 4.9 us
    all_gather x3 -> x0, waiting for transfers between devices: 77.1 us -> none  [the longest x2 48.4 us: sent_together(): lax.all_gather(both, axis, axis=dim, tiled=True)]
    pallas_call x0 -> x1, Pallas kernels: none -> 63.6 us  [local(): pl.pallas_call(kernel, out_shape=jax.ShapeDtypeStruct((BLOCK, D), BF16),...]
    reduce_scatter x1 -> x0, waiting for transfers between devices: 35.3 us -> none  [local(): lax.psum_scatter((jnp.dot(attended, out_attend, preferred_element_type=jn...]
    dot_general x8 -> x0, matrix products: 22.4 us -> none  [the longest x4 10.1 us: local(): jnp.dot(all_rows, weight_piece, preferred_element_type=jnp.float32)]
    ppermute x3 -> x0, starting transfers between devices: 10.4 us -> none  [passed_along(): return lax.ppermute(block, axis, route)]
    all_to_all x1 -> x0, starting transfers between devices: 6.14 us -> none  [from_everyone(): return lax.all_to_all(copies, axis, split_axis=0, concat_axis=0, tiled=True)]
    concatenate x5 -> x0, other arithmetic: 3.81 us -> none  [the longest x2 2.15 us: sent_together(): both = jnp.concatenate(arrays, axis=along)]
    slice x12 -> x0, local copies, waits for them, and re-layouts: 3.74 us -> none  [the longest x4 0.93 us: local(): key_pairs = jnp.concatenate([key_ext[:-1], key_ext[1:]], axis=1)]
  transfers between devices with their start and end apart: 8 -> 0, of which waited for: 4 -> 0; matrix products, arithmetic and copies ran while one was open for 17% -> 0% of each run, Pallas kernels for 0% -> 0%
where the time goes in v1:
time: 68.9 us; the launch traced here: 68.5 us
  Pallas kernels  63.6 us (92%)
  local copies, waits for them, and re-layouts  4.9 us (7%)
    pallas_call x1, Pallas kernels, local(): pl.pallas_call(kernel, out_shape=jax.ShapeDtypeStruct((BLOCK, D), BF16),...  63.6 us
    unnamed x19, local copies, waits for them, and re-layouts  4.9 us

profile of v1, /device:TPU:0, one launch (start us, length us, event | category | flops | bytes accessed | tf_op | source)
XLA Modules:
  0.0 68.5 jit_solution(15602301275633296853)
XLA Ops:
  0.0 0.0 copy-start.6
  0.0 0.0 copy-start.7
  0.0 0.0 copy-start.2
  0.0 0.0 copy-start.3
  0.0 0.9 %copy.11.wk_hbm = bf16[128,64]{1,0:T(8,128)(2,1)S(1)} copy(bf16[128,64]{0,1:T(8,128)(2,1)} %param.13) | data formatting | bytes 32768 | tf_op args[3]
  0.9 0.0 copy-start.1
  0.9 0.8 %copy.12.wv_hbm = bf16[128,64]{1,0:T(8,128)(2,1)S(1)} copy(bf16[128,64]{0,1:T(8,128)(2,1)} %param.14) | data formatting | bytes 32768 | tf_op args[4]
  1.7 0.0 copy-done.6
  1.7 0.0 copy-done.7
  1.7 0.0 copy-done.2
  1.7 0.0 copy-done.3
  1.8 0.0 copy-done.1
  1.8 0.0 copy-start
  1.8 1.0 %copy-done = bf16[96,2048]{1,0:T(8,128)(2,1)S(1)} copy-done((bf16[96,2048]{1,0:T(8,128)(2,1)S(1)}, bf16[96,2048]{1,0:T(8,128)(2,1)}, u32[]{:S(2)}) %copy-start) | copy-done | bytes 393240
  2.8 0.0 copy-start.4
  2.8 0.8 %copy-done.4 = bf16[128,128]{1,0:T(8,128)(2,1)S(1)} copy-done((bf16[128,128]{1,0:T(8,128)(2,1)S(1)}, bf16[128,128]{1,0:T(8,128)(2,1)}, u32[]{:S(2)}) %copy-start.4) | copy-done | bytes 32792
  3.5 0.0 copy-start.5
  3.5 0.7 %copy-done.5 = f32[2048]{0:T(1024)S(1)} copy-done((f32[2048]{0:T(1024)S(1)}, f32[2048]{0:T(1024)}, u32[]{:S(2)}) %copy-start.5) | copy-done | bytes 8216
  4.2 63.6 %shard_map.100 = bf16[96,2048]{1,0:T(8,128)(2,1)S(1)} custom-call(bf16[96,2048]{1,0:T(8,128)(2,1)S(1)} %copy-done, f32[1,2048]{1,0:T(1,128)S(1)} %bitcast.2, bf16[128,128]{1,0:T(8,128)(2,1)S(1)} %copy-done.1, bf16[128,64]{1,0:T(8,128)(2,1)S(1)} %copy.11.wk_hbm, bf16[128,64]{1,0:T(8,128)(2,1)S(1)} %copy.12.wv_hbm, bf16[128,128]{1,0:T(8,128)(2,1)S(1)} %copy-done.2, ...), custom_call_target="tpu_custom_call" | custom-call | tf_op jit(solution)/shard_map/pallas_call | solution.py:538
  67.8 0.7 %copy.14 = bf16[96,2048]{1,0:T(8,128)(2,1)} copy(bf16[96,2048]{1,0:T(8,128)(2,1)S(1)} %shard_map.100) | data formatting | bytes 786432
Async XLA Ops:
  0.0 1.7 %copy-start.6 = (f32[2]{0:T(128)S(1)}, f32[2]{0:T(128)}, u32[]{:S(2)}) copy-start(f32[2]{0:T(128)} %sink_ref.1) | copy-start | bytes 28
  0.0 1.7 %copy-start.7 = (f32[128]{0:T(128)S(1)}, f32[128]{0:T(128)}, u32[]{:S(2)}) copy-start(f32[128]{0:T(128)} %param.17) | copy-start | bytes 1540
  0.0 1.7 %copy-start.2 = (bf16[128,128]{1,0:T(8,128)(2,1)S(1)}, bf16[128,128]{1,0:T(8,128)(2,1)}, u32[]{:S(2)}) copy-start(bf16[128,128]{1,0:T(8,128)(2,1)} %wp_hbm.1) | copy-start | bytes 98308
  0.0 1.7 %copy-start.3 = (bf16[128,128]{1,0:T(8,128)(2,1)S(1)}, bf16[128,128]{1,0:T(8,128)(2,1)}, u32[]{:S(2)}) copy-start(bf16[128,128]{1,0:T(8,128)(2,1)} %wa_hbm.1) | copy-start | bytes 98308
  0.9 0.9 %copy-start.1 = (bf16[128,128]{1,0:T(8,128)(2,1)S(1)}, bf16[128,128]{1,0:T(8,128)(2,1)}, u32[]{:S(2)}) copy-start(bf16[128,128]{1,0:T(8,128)(2,1)} %wq_hbm.1) | copy-start | bytes 98308
  1.8 1.0 %copy-start = (bf16[96,2048]{1,0:T(8,128)(2,1)S(1)}, bf16[96,2048]{1,0:T(8,128)(2,1)}, u32[]{:S(2)}) copy-start(bf16[96,2048]{1,0:T(8,128)(2,1)} %x_hbm.1) | copy-start | bytes 1179652
  2.8 0.8 %copy-start.4 = (bf16[128,128]{1,0:T(8,128)(2,1)S(1)}, bf16[128,128]{1,0:T(8,128)(2,1)}, u32[]{:S(2)}) copy-start(bf16[128,128]{1,0:T(8,128)(2,1)} %wo_hbm.1) | copy-start | bytes 98308
  3.5 0.7 %copy-start.5 = (f32[2048]{0:T(1024)S(1)}, f32[2048]{0:T(1024)}, u32[]{:S(2)}) copy-start(f32[2048]{0:T(1024)} %param.11) | copy-start | bytes 24580

commit v2 on v1

--- a/solution.py
+++ b/solution.py
@@ -80,8 +80,7 @@
     xin,
     gain,
     pgain,
-    wk,
-    wv,
+    wkv,
     tok,
     win,
     wout,
@@ -124,13 +123,20 @@
     partner = (sp, y * 2 + other)
     up, down = (sp, yn * 2 + c), (sp, yp * 2 + c)
 
+    barrier = pltpu.get_barrier_semaphore()
+    beside = [(z * SIDE + turn(x, by), tp) for by in (1, -1)]
+    above = [(turn(z, by) * SIDE + x, tp) for by in (1, -1)]
+    peers = [up, down, partner] + beside + above
+    for peer in peers:
+        pl.semaphore_signal(barrier, inc=1, device_id=peer, device_id_type=MESH)
+
     own_in = rows_of(sp * DEPTH, DEPTH, 128)
     own_cols = rows_of(sp * 128, 128, 128)
     loads = [
         (x_hbm, xin),
         (gain_hbm, gain),
-        (wk_hbm, wk),
-        (wv_hbm, wv),
+        (wk_hbm, wkv.at[pl.ds(0, HEAD_DIM)]),
+        (wv_hbm, wkv.at[pl.ds(HEAD_DIM, HEAD_DIM)]),
         (wq_hbm, win.at[own_in, pl.ds(0, 128)]),
         (wp_hbm, win.at[own_in, pl.ds(256, 128)]),
         (pgain_hbm, pgain),
@@ -141,13 +147,6 @@
     for load in loads:
         load.start()
 
-    barrier = pltpu.get_barrier_semaphore()
-    for step in range(1, PLANE):
-        peer = (lax.rem(sp + step, PLANE), tp)
-        pl.semaphore_signal(barrier, inc=1, device_id=peer, device_id_type=MESH)
-    for peer in (up, down, partner):
-        pl.semaphore_signal(barrier, inc=1, device_id=peer, device_id_type=MESH)
-
     loads[0].wait()
     loads[1].wait()
     gains = gain[...]
@@ -157,11 +156,12 @@
         tok[rows_of(tp * BLOCK + r, 16), :] = (wide * inverse * gains).astype(BF16)
     loads[2].wait()
     loads[3].wait()
-    win[own_in, pl.ds(128, 128)] = jnp.concatenate([wk[...], wv[...]], axis=1)
+    win[own_in, pl.ds(128, 128)] = wkv[...].T
     for load in loads[4:]:
         load.wait()
 
     messages = Messages(send_sems, recv_sems)
+
 
     def block(yy, cc):
         return tok.at[rows_of((yy * 2 + cc) * BLOCK, BLOCK)]
@@ -260,46 +260,47 @@
         wout.at[pl.ds(0, 256)], wout.at[pl.ds(256, 256)], partner, wout.at[pl.ds(256, 256)]
     )
 
-    pl.semaphore_wait(barrier, PLANE - 1 + 3)
+    pl.semaphore_wait(barrier, len(peers))
 
     for m in (t_n0, t_p1, t_n1, t_p0):
         m.start()
-    for g in ins:
+    for g in ins + outs:
         g.begin()
     d_own.start()
     for g in ins:
+        g.near()
+    for g in outs:
         g.near()
     for g in ins:
         g.pass_on(0)
     for g in ins:
         g.distant()
+    for g in ins:
+        g.pass_on(-1)
+        g.pass_on(1)
     t_n0.arrived()
     f_n.start()
     d_p0.start()
     t_p1.arrived()
     f_p.start()
     d_n1.start()
-    for g in ins:
-        g.pass_on(-1)
-        g.pass_on(1)
-    for g in ins:
-        g.pass_on(2)
-    for g in outs:
-        g.begin()
-    for g in outs:
-        g.near()
     for g in outs:
         g.pass_on(0)
     for g in outs:
         g.distant()
     for g in ins:
-        g.finish()
+        g.pass_on(2)
+    for g in outs:
+        g.pass_on(-1)
+        g.pass_on(1)
     t_n1.arrived()
     d_p1.start()
     t_p0.arrived()
     d_n0.start()
-
-    lane = lax.broadcasted_iota(jnp.int32, (CHUNK, 128), 1)
+    for g in ins:
+        g.finish()
+    for g in outs:
+        g.pass_on(2)
 
     def spread(kv, rows, at):
         first = lax.broadcasted_iota(jnp.int32, (rows, 128), 1) < HEAD_DIM
@@ -321,20 +322,12 @@
 
     d_own.arrived()
     total = project(y)
-    for g in outs:
-        g.pass_on(-1)
-        g.pass_on(1)
     d_p0.arrived()
     d_p1.arrived()
     total = total + project(yp)
-    for g in outs:
-        g.pass_on(2)
     d_n0.arrived()
     d_n1.arrived()
     total = total + project(yn)
-    for g in outs:
-        g.finish()
-    d_out.start()
     f_n.arrived()
     d_f0.start()
     f_p.arrived()
@@ -342,6 +335,9 @@
     d_f0.arrived()
     d_f1.arrived()
     total = total + project(yf)
+    for g in outs:
+        g.finish()
+    d_out.start()
 
     last = pl.ds(ROWS, WINDOW)
     kvsend[...] = kp0[last, :] + vp1[last, :]
@@ -502,13 +498,12 @@
     attention_out_weight,
     pool_out_weight,
 ):
-    hbm = pl.BlockSpec(memory_space=pl.ANY)
+    hbm = pl.BlockSpec(memory_space=pltpu.HBM)
     scratch = [
         ((BLOCK, D), BF16),
         ((1, D), F32),
         ((1, 128), F32),
-        ((DEPTH, 64), BF16),
-        ((DEPTH, 64), BF16),
+        ((DEPTH, DEPTH), BF16),
         ((ROWS, D), BF16),
         ((D, IN_COLS), BF16),
         ((512, D), BF16),
@@ -547,14 +542,14 @@
             pltpu.SemaphoreType.DMA((N_MSG,)),
         ],
         compiler_params=pltpu.CompilerParams(
-            collective_id=0, has_side_effects=True, vmem_limit_bytes=40 * 1024 * 1024
+            collective_id=0, has_side_effects=True, vmem_limit_bytes=62 * 1024 * 1024
         ),
     )(
         tokens_in,
         norm_gain.reshape(1, D),
         query_weight,
-        key_weight,
-        value_weight,
+        key_weight.T,
+        value_weight.T,
         pool_weight,
         sink_logit,
         pool_gain.reshape(1, 128),

time: 68.9 us -> 57.4 us (0.83)
  the two profiles are of different devices: /device:TPU:0 before, /device:TPU:1 now
where the time goes in v2:
time: 57.4 us; the launch traced here: 57.2 us
  Pallas kernels  55.5 us (97%)
  local copies, waits for them, and re-layouts  1.77 us (3%)
    pallas_call x1, Pallas kernels, local(): pl.pallas_call(kernel, out_shape=jax.ShapeDtypeStruct((BLOCK, D), BF16),...  55.5 us
    unnamed x1, local copies, waits for them, and re-layouts  1.77 us

profile of v2, /device:TPU:1, one launch (start us, length us, event | category | flops | bytes accessed | tf_op | source)
XLA Modules:
  0.0 57.2 jit_solution(13831621546702070642)
XLA Ops:
  0.0 55.5 %shard_map.100 = bf16[96,2048]{1,0:T(8,128)(2,1)} custom-call(bf16[96,2048]{1,0:T(8,128)(2,1)} %x_hbm.1, f32[1,2048]{1,0:T(1,128)} %bitcast.6, bf16[128,128]{1,0:T(8,128)(2,1)} %wq_hbm.1, bf16[64,128]{1,0:T(8,128)(2,1)} %bitcast.4, bf16[64,128]{1,0:T(8,128)(2,1)} %bitcast.5, bf16[128,128]{1,0:T(8,128)(2,1)} %wp_hbm.1, f32[2]{0:T(128)} %sink_ref.1, ...), custom_call_target="tpu_custom_call" | custom-call | tf_op jit(solution)/shard_map/pallas_call | solution.py:533
  55.5 1.8 %copy.12 = bf16[96,2048]{1,0:T(8,128)(2,1)} copy(bf16[96,2048]{1,0:T(8,128)(2,1)} %shard_map.100) | data formatting | bytes 786432

commit v3 on v2

v3 whole, which is shorter than its diff:
```python
import jax
import jax.numpy as jnp
from jax import lax
from jax.experimental import pallas as pl
from jax.experimental.pallas import tpu as pltpu
from jax.sharding import PartitionSpec as P

MESH = pl.DeviceIdType.MESH
F32 = jnp.float32
BF16 = jnp.bfloat16

D = 2048
HEAD_DIM = 64
WINDOW = 128
EPS = 1e-06
SIDE = 4
PLANE = SIDE * SIDE
BLOCK = 96
HALF = BLOCK // 2
ROWS = 2 * SIDE * BLOCK
CHUNK = 2 * BLOCK
DEPTH = D // PLANE
IN_COLS = 384
N_GROUPS = 40


class Groups:
    def __init__(self, send_sems, recv_sems):
        self.send_sems, self.recv_sems, self.made = send_sems, recv_sems, []

    def new(self, whole):
        group = Group(self.send_sems.at[len(self.made)], self.recv_sems.at[len(self.made)], whole)
        self.made.append(group)
        return group

    def one(self, src, dst, device, land):
        group = self.new(land)
        group.add(src, dst, device)
        return group


class Group:
    def __init__(self, send_sem, recv_sem, whole):
        self.send_sem, self.recv_sem, self.whole, self.copies = send_sem, recv_sem, whole, []

    def copy(self, src, dst, device):
        return pltpu.make_async_remote_copy(
            src_ref=src,
            dst_ref=dst,
            send_sem=self.send_sem,
            recv_sem=self.recv_sem,
            device_id=device,
            device_id_type=MESH,
        )

    def add(self, src, dst, device):
        self.device = device
        self.copies.append((src, dst, device))
        return len(self.copies) - 1

    def start(self, *which):
        for n in which or range(len(self.copies)):
            self.copy(*self.copies[n]).start()

    def arrived(self):
        self.copy(self.whole, self.whole, self.device).wait_recv()

    def sent(self):
        self.copy(self.whole, self.whole, self.device).wait_send()


def rows_of(start, size, unit=16):
    return pl.ds(pl.multiple_of(start, unit), size)


def kernel(
    x_hbm,
    gain_hbm,
    wq_hbm,
    wk_hbm,
    wv_hbm,
    wp_hbm,
    sink_hbm,
    pgain_hbm,
    wa_hbm,
    wo_hbm,
    out_ref,
    xin,
    gain,
    pgain,
    sink,
    wkv,
    tok,
    win,
    wout,
    qbuf,
    kvsend,
    kvland,
    kp0,
    kp1,
    vp0,
    vp1,
    pext,
    totals,
    before,
    cols_own,
    cols_y,
    cols_core,
    cols_other,
    cols_sp,
    amine,
    apart,
    far,
    nbn,
    nbp,
    accn,
    accp,
    rfn,
    rfp,
    rn,
    rp,
    local_sems,
    send_sems,
    recv_sems,
):
    sp = lax.axis_index("sp")
    tp = lax.axis_index("tp")
    z, x = sp // SIDE, lax.rem(sp, SIDE)
    y, c = tp // 2, lax.rem(tp, 2)
    other = 1 - c

    def turn(i, by):
        return lax.rem(i + by + SIDE, SIDE)

    yn, yp, yf = turn(y, 1), turn(y, -1), turn(y, 2)
    partner = (sp, y * 2 + other)
    up, down = (sp, yn * 2 + c), (sp, yp * 2 + c)

    barrier = pltpu.get_barrier_semaphore()
    beside = [(z * SIDE + turn(x, by), tp) for by in (1, -1)]
    above = [(turn(z, by) * SIDE + x, tp) for by in (1, -1)]
    opposite = [(z * SIDE + turn(x, 2), tp), (turn(z, 2) * SIDE + x, tp), (sp, yf * 2 + c)]
    peers = [up, down, partner] + beside + above + opposite
    for peer in peers:
        pl.semaphore_signal(barrier, inc=1, device_id=peer, device_id_type=MESH)

    own_in = rows_of(sp * DEPTH, DEPTH, 128)
    own_cols = rows_of(sp * 128, 128, 128)
    loads = [
        (0, x_hbm, xin),
        (1, gain_hbm, gain),
        (2, wk_hbm, wkv.at[pl.ds(0, HEAD_DIM)]),
        (2, wv_hbm, wkv.at[pl.ds(HEAD_DIM, HEAD_DIM)]),
        (3, wq_hbm, win.at[own_in, pl.ds(0, 128)]),
        (3, wp_hbm, win.at[own_in, pl.ds(256, 128)]),
        (4, wa_hbm, wout.at[pl.ds(0, 128), own_cols]),
        (4, wo_hbm, wout.at[pl.ds(128, 128), own_cols]),
        (5, pgain_hbm, pgain),
        (6, sink_hbm, sink),
    ]
    for n, src, dst in loads:
        pltpu.make_async_copy(src, dst, local_sems.at[n]).start()

    def loaded(n, whole):
        pltpu.make_async_copy(whole, whole, local_sems.at[n]).wait()

    loaded(0, xin)
    loaded(1, gain)
    gains = gain[...]

    def column_sums(rows):
        return jnp.sum(rows.astype(F32), axis=0, keepdims=True)

    columns = jnp.zeros((1, D), F32)
    for r in range(0, BLOCK, 16):
        wide = xin[pl.ds(r, 16)].astype(F32)
        inverse = lax.rsqrt(jnp.mean(wide * wide, axis=1, keepdims=True) + EPS)
        normed = (wide * inverse * gains).astype(BF16)
        tok[rows_of(tp * BLOCK + r, 16), :] = normed
        columns = columns + column_sums(normed)
    cols_own[...] = columns
    loaded(2, wkv)
    win[own_in, pl.ds(128, 128)] = wkv[...].T
    loaded(3, win.at[own_in, pl.ds(0, 256)])
    loaded(4, wout.at[pl.ds(0, 256), own_cols])
    loaded(5, pgain)
    loaded(6, sink)

    groups = Groups(send_sems, recv_sems)

    def block(yy, cc):
        return tok.at[rows_of((yy * 2 + cc) * BLOCK, BLOCK)]

    def half(yy, cc, h):
        return tok.at[rows_of((yy * 2 + cc) * BLOCK + h * HALF, HALF)]

    one = groups.one
    c_y = groups.new(cols_y)
    for n, by in enumerate((1, -1, 2)):
        c_y.add(cols_own, cols_y.at[n], (sp, turn(y, by) * 2 + c))
    t_n0 = one(half(y, c, 0), half(y, c, 0), up, half(yp, c, 0))
    t_p1 = one(half(y, c, 1), half(y, c, 1), down, half(yn, c, 1))
    t_n1 = one(half(y, c, 1), half(y, c, 1), up, half(yp, c, 1))
    t_p0 = one(half(y, c, 0), half(y, c, 0), down, half(yn, c, 0))
    f_n = one(half(yp, c, 0), half(yp, c, 0), up, half(yf, c, 0))
    f_p = one(half(yn, c, 1), half(yn, c, 1), down, half(yf, c, 1))
    d_own = one(block(y, c), block(y, c), partner, block(y, other))

    def across(yy):
        group = groups.new(block(yy, other))
        for h in range(2):
            group.add(half(yy, c, h), half(yy, c, h), partner)
        return group

    d_p, d_n, d_f = across(yp), across(yn), across(yf)
    c_core = one(cols_core, cols_other, partner, cols_other)
    c_sp = groups.new(cols_sp.at[pl.ds(0, PLANE - 1)])
    for step in range(1, PLANE):
        c_sp.add(cols_sp.at[sp], cols_sp.at[sp], (lax.rem(sp + step, PLANE), tp))

    class Gather:
        def __init__(self, piece, sub, whole, direct, crossing_direct, shared=None):
            def source(g, o1, o2):
                if g == 0:
                    return turn(z, o2) * SIDE + turn(x, o1)
                return turn(z, o1) * SIDE + turn(x, o2)

            def put(group, ref, g, o1, o2):
                return group.add(ref, ref, (source(g, o1, o2), tp))

            self.first = groups.new(whole(4))
            self.first_far = groups.new(whole(2))
            self.last = groups.new(whole(8))
            self.direct = direct
            self.second, self.forward = {}, {}
            for g in range(2):
                mine = piece(g, source(g, 0, 0))
                put(self.first, mine, g, 1, 0)
                put(self.first, mine, g, -1, 0)
                if direct:
                    put(self.first_far, mine, g, 2, 0)
                else:
                    put(self.first_far, sub(g, source(g, -1, 0), 0), g, 1, 0)
                    put(self.first_far, sub(g, source(g, 1, 0), 1), g, -1, 0)
            for o in (0, -1, 1, 2):
                self.second[o] = groups.new(whole(4))
                self.forward[o] = []
                for g in range(2):
                    have = piece(g, source(g, o, 0))
                    put(self.second[o], have, g, 0, 1)
                    put(self.second[o], have, g, 0, -1)
                    if o in crossing_direct:
                        self.forward[o].append(put(self.last, have, g, 0, 2))
                    else:
                        low, high = sub(g, source(g, o, -1), 0), sub(g, source(g, o, 1), 1)
                        self.forward[o].append(put(self.last, low, g, 0, 1))
                        self.forward[o].append(put(self.last, high, g, 0, -1))
            self.crossing_direct = crossing_direct
            self.shares = None
            if shared:
                self.shares = groups.new(shared[0])
                self.share_of = {}
                for o1 in (0, -1, 1, 2):
                    for o2 in (0, -1, 1, 2):
                        self.share_of[o1, o2] = [
                            self.shares.add(
                                piece(g, source(g, o1, o2)), shared[1](g, source(g, o1, o2)), partner
                            )
                            for g in range(2)
                        ]

        def share(self, o1, o2):
            if self.shares:
                self.shares.start(*self.share_of[o1, o2])

        def begin(self):
            self.first.start()
            if self.direct:
                self.first_far.start()

        def cross(self, o):
            self.second[o].start()
            if o in self.crossing_direct:
                self.last.start(*self.forward[o])
            self.share(o, 0)

        def near(self):
            self.first.arrived()
            if not self.direct:
                self.first_far.start()
            self.cross(-1)
            self.cross(1)

        def distant(self):
            self.first_far.arrived()
            self.cross(2)

        def pass_on(self, o):
            self.second[o].arrived()
            if o not in self.crossing_direct:
                self.last.start(*self.forward[o])
            self.share(o, -1)
            self.share(o, 1)

        def finish(self):
            self.last.arrived()
            for o in (0, -1, 1, 2):
                self.share(o, 2)

    size = DEPTH // 2
    ins = Gather(
        lambda g, s: win.at[rows_of(s * DEPTH + g * size, size)],
        lambda g, s, h: win.at[rows_of(s * DEPTH + g * size + h * (size // 2), size // 2)],
        lambda n: win.at[pl.ds(0, n * size)],
        True,
        (),
    )
    outs = Gather(
        lambda g, s: wout.at[pl.ds(g * 128, 128), rows_of(s * 128, 128, 128)],
        lambda g, s, h: wout.at[pl.ds(g * 128 + h * 64, 64), rows_of(s * 128, 128, 128)],
        lambda n: wout.at[pl.ds(0, n * 8)],
        False,
        (2,),
        (
            wout.at[pl.ds(256, 256)],
            lambda g, s: wout.at[pl.ds(256 + g * 128, 128), rows_of(s * 128, 128, 128)],
        ),
    )

    pl.semaphore_wait(barrier, len(peers))

    for group in (c_y, t_n0, t_p1, t_n1, t_p0):
        group.start()
    ins.begin()
    outs.begin()
    ins.cross(0)
    outs.cross(0)
    d_own.start()
    ins.near()
    ins.distant()
    c_y.arrived()
    own_parity = columns + cols_y[0] + cols_y[1] + cols_y[2]
    cols_core[...] = own_parity
    c_core.start()
    outs.near()
    ins.pass_on(0)
    c_core.arrived()
    cols_sp[sp] = own_parity + cols_other[...]

    @pl.when(y == SIDE - 1)
    def _():
        c_sp.start()

    t_n0.arrived()
    f_n.start()
    d_p.start(0)
    t_p1.arrived()
    f_p.start()
    d_n.start(1)
    outs.pass_on(0)
    ins.pass_on(-1)
    ins.pass_on(1)
    ins.pass_on(2)
    outs.distant()
    t_n1.arrived()
    d_p.start(1)
    t_p0.arrived()
    d_n.start(0)
    outs.pass_on(-1)
    outs.pass_on(1)
    ins.finish()

    def spread(kv, rows, at):
        first = lax.broadcasted_iota(jnp.int32, (rows, 128), 1) < HEAD_DIM
        turned = pltpu.roll(kv, HEAD_DIM, 1)
        kp0[at, :] = jnp.where(first, kv, 0.0).astype(BF16)
        kp1[at, :] = jnp.where(first, 0.0, turned).astype(BF16)
        vp0[at, :] = jnp.where(first, turned, 0.0).astype(BF16)
        vp1[at, :] = jnp.where(first, 0.0, kv).astype(BF16)

    last = pl.ds(ROWS, WINDOW)
    after = (lax.rem(sp + 1, PLANE), tp)
    halo = groups.new(pext.at[pl.ds(0, 2 * WINDOW)])
    halo.add(kvsend, kvland, after)
    halo.add(pext.at[last], pext.at[pl.ds(0, WINDOW)], after)

    def project(yy):
        at = rows_of(yy * CHUNK, CHUNK)
        got = jnp.dot(tok[at, :], win[...], preferred_element_type=F32)
        qbuf[at, :] = got[:, :128].astype(BF16)
        ahead = rows_of(yy * CHUNK + WINDOW, CHUNK)
        spread(got[:, 128:256].astype(BF16).astype(F32), CHUNK, ahead)
        pool = got[:, 256:].astype(BF16)
        pext[ahead, :] = pool
        sums = jnp.sum(pool.astype(F32).reshape(2, BLOCK // 8, 8, 128), axis=1)
        totals[pl.ds(yy * 2, 2)] = sums

        @pl.when(yy == SIDE - 1)
        def _():
            kvsend[...] = kp0[last, :] + vp1[last, :]
            halo.start()

    f_n.arrived()
    d_f.start(0)
    f_p.arrived()
    d_f.start(1)
    d_own.arrived()
    project(y)
    d_p.arrived()
    project(yp)
    d_n.arrived()
    project(yn)
    outs.pass_on(2)
    d_f.arrived()
    project(yf)
    outs.finish()

    @pl.when(y == SIDE - 1)
    def _():
        c_sp.arrived()
        earlier = lax.broadcasted_iota(jnp.int32, (PLANE, 1, D), 0) < sp
        ahead = jnp.sum(jnp.where(earlier, cols_sp[...], 0.0), axis=0)
        high = ahead.astype(BF16).astype(F32)
        middle = (ahead - high).astype(BF16).astype(F32)
        low = ahead - high - middle
        term = lax.broadcasted_iota(jnp.int32, (16, D), 0)
        terms = jnp.where(term == 0, high, jnp.where(term == 1, middle, jnp.where(term == 2, low, 0.0)))
        got = jnp.dot(terms.astype(BF16), win[:, 256:], preferred_element_type=F32)
        before[...] = jnp.sum(got, axis=0, keepdims=True)

    span = WINDOW + BLOCK
    q_index = lax.broadcasted_iota(jnp.int32, (BLOCK, span), 0)
    k_index = lax.broadcasted_iota(jnp.int32, (BLOCK, span), 1)
    distance = q_index + WINDOW - k_index
    reach = jnp.where(y == 0, 8, jnp.where(y == 1, 32, jnp.where(y == 2, WINDOW, 1 << 24)))
    inside = (distance >= 0) & (distance < WINDOW)
    banded = (distance >= 0) & (distance < reach) & ((k_index >= WINDOW) | (y < 3))
    sinks = (sink[:, 0:1], sink[:, 1:2])
    pool_gain = pgain[...]

    def probabilities(q, keys, allowed, sink):
        scores = lax.dot_general(q, keys, (((1,), (1,)), ((), ())), preferred_element_type=F32)
        scores = jnp.where(allowed, scores * HEAD_DIM ** (-0.5), -jnp.inf)
        peak = jnp.maximum(jnp.max(scores, axis=1, keepdims=True), sink)
        expo = jnp.exp(scores - peak)
        denom = jnp.sum(expo, axis=1, keepdims=True) + jnp.exp(sink - peak)
        return (expo * (1.0 / denom)).astype(BF16)

    def attend(yy, cc):
        number = yy * 2 + cc
        start = sp * ROWS + number * BLOCK
        at, pair = rows_of(number * BLOCK, BLOCK), rows_of(number * BLOCK, span)
        present = k_index >= WINDOW - start
        allowed, band = inside & present, banded & present
        q = qbuf[at, :]
        p0 = probabilities(q, kp0[pair, :], allowed, sinks[0])
        p1 = probabilities(q, kp1[pair, :], allowed, sinks[1])
        mixed = jnp.dot(p0, vp0[pair, :], preferred_element_type=F32)
        mixed = mixed + jnp.dot(p1, vp1[pair, :], preferred_element_type=F32)
        amine[at, pl.ds(0, 128)] = mixed.astype(BF16)
        ones = jnp.where(band, 1.0, 0.0).astype(BF16)
        sums = jnp.dot(ones, pext[pair, :], preferred_element_type=F32)
        earlier = lax.broadcasted_iota(jnp.int32, (2 * SIDE, 8, 128), 0) < number
        carry = jnp.sum(jnp.sum(jnp.where(earlier, totals[...], 0.0), axis=0), axis=0, keepdims=True)
        carry = jnp.where(y == 3, carry + before[...], 0.0)
        position = start + lax.broadcasted_iota(jnp.int32, (BLOCK, 128), 0)
        count = jnp.minimum(position + 1, reach).astype(F32)
        value = pext[rows_of(number * BLOCK + WINDOW, BLOCK), :].astype(F32)
        pooled = (sums + carry) / count
        amine[at, pl.ds(128, 128)] = ((pooled - value) * pool_gain).astype(BF16)

    def first_half(yy):
        @pl.when(yy == 0)
        def _():
            halo.arrived()
            spread(kvland[...].astype(F32), WINDOW, pl.ds(0, WINDOW))

        attend(yy, other)
        src = amine.at[rows_of((yy * 2 + other) * BLOCK, BLOCK)]
        dst = apart.at[rows_of(yy * BLOCK, BLOCK)]
        swap = one(src, dst, partner, dst)
        swap.start()
        return swap

    def product(yy, put):
        mine = amine[rows_of((yy * 2 + c) * BLOCK, BLOCK), :]
        theirs = apart[rows_of(yy * BLOCK, BLOCK), :]
        for n in range(0, D, 512):
            cols = pl.ds(n, 512)
            got = jnp.dot(mine, wout[pl.ds(0, 256), cols], preferred_element_type=F32)
            got = got + jnp.dot(theirs, wout[pl.ds(256, 256), cols], preferred_element_type=F32)
            put(cols, got)

    top, bottom = pl.ds(0, HALF), pl.ds(HALF, HALF)
    r_fn = one(far.at[top], rfn, up, rfn)
    r_fp = one(far.at[bottom], rfp, down, rfp)
    r_n1 = one(nbn.at[bottom], rn.at[bottom], up, rn.at[bottom])
    r_p0 = one(nbp.at[top], rp.at[top], down, rp.at[top])
    r_n0 = one(nbn.at[top], rn.at[top], up, rn.at[top])
    r_p1 = one(nbp.at[bottom], rp.at[bottom], down, rp.at[bottom])

    def put_far(cols, got):
        far[:, cols] = got.astype(BF16)

    def put_next(cols, got):
        nbn[bottom, cols] = got[HALF:].astype(BF16)
        accn[:, cols] = got[:HALF]

    def put_prev(cols, got):
        nbp[top, cols] = got[:HALF].astype(BF16)
        accp[:, cols] = got[HALF:]

    swap_f = first_half(yf)
    attend(yf, c)
    swap_n = first_half(yn)
    outs.shares.arrived()
    swap_f.arrived()
    product(yf, put_far)
    r_fn.start()
    r_fp.start()
    attend(yn, c)
    swap_p = first_half(yp)
    swap_n.arrived()
    product(yn, put_next)
    r_n1.start()
    attend(yp, c)
    swap_o = first_half(y)
    swap_p.arrived()
    product(yp, put_prev)
    r_p0.start()
    attend(y, c)
    r_fn.arrived()
    nbn[top, :] = (accn[...] + rfn[...].astype(F32)).astype(BF16)
    r_n0.start()
    r_fp.arrived()
    nbp[bottom, :] = (accp[...] + rfp[...].astype(F32)).astype(BF16)
    r_p1.start()
    swap_o.arrived()

    def put_own(cols, got):
        accn[:, cols] = got[:HALF]
        accp[:, cols] = got[HALF:]

    product(y, put_own)
    r_n1.arrived()
    accp[...] = accp[...] + rn[bottom, :].astype(F32)
    r_p0.arrived()
    accn[...] = accn[...] + rp[top, :].astype(F32)
    r_n0.arrived()
    out_ref[top, :] = (accn[...] + rn[top, :].astype(F32)).astype(BF16)
    r_p1.arrived()
    out_ref[bottom, :] = (accp[...] + rp[bottom, :].astype(F32)).astype(BF16)
    for group in groups.made:
        if group is not c_sp:
            group.sent()

    @pl.when(y == SIDE - 1)
    def _():
        c_sp.sent()

    assert len(groups.made) <= N_GROUPS


def local(
    tokens_in,
    norm_gain,
    query_weight,
    key_weight,
    value_weight,
    pool_weight,
    sink_logit,
    pool_gain,
    attention_out_weight,
    pool_out_weight,
):
    hbm = pl.BlockSpec(memory_space=pltpu.HBM)
    scratch = [
        ((BLOCK, D), BF16),
        ((1, D), F32),
        ((1, 128), F32),
        ((1, 2), F32),
        ((DEPTH, DEPTH), BF16),
        ((ROWS, D), BF16),
        ((D, IN_COLS), BF16),
        ((512, D), BF16),
        ((ROWS, 128), BF16),
        ((WINDOW, 128), BF16),
        ((WINDOW, 128), BF16),
        ((ROWS + WINDOW, 128), BF16),
        ((ROWS + WINDOW, 128), BF16),
        ((ROWS + WINDOW, 128), BF16),
        ((ROWS + WINDOW, 128), BF16),
        ((ROWS + WINDOW, 128), BF16),
        ((2 * SIDE, 8, 128), F32),
        ((1, 128), F32),
        ((1, D), F32),
        ((3, 1, D), F32),
        ((1, D), F32),
        ((1, D), F32),
        ((PLANE, 1, D), F32),
        ((ROWS, 256), BF16),
        ((SIDE * BLOCK, 256), BF16),
        ((BLOCK, D), BF16),
        ((BLOCK, D), BF16),
        ((BLOCK, D), BF16),
        ((HALF, D), F32),
        ((HALF, D), F32),
        ((HALF, D), BF16),
        ((HALF, D), BF16),
        ((BLOCK, D), BF16),
        ((BLOCK, D), BF16),
    ]
    return pl.pallas_call(
        kernel,
        out_shape=jax.ShapeDtypeStruct((BLOCK, D), BF16),
        in_specs=[hbm] * 10,
        out_specs=pl.BlockSpec(memory_space=pltpu.VMEM),
        scratch_shapes=[pltpu.VMEM(shape, kind) for shape, kind in scratch]
        + [
            pltpu.SemaphoreType.DMA((7,)),
            pltpu.SemaphoreType.DMA((N_GROUPS,)),
            pltpu.SemaphoreType.DMA((N_GROUPS,)),
        ],
        compiler_params=pltpu.CompilerParams(
            collective_id=0, has_side_effects=True, vmem_limit_bytes=62 * 1024 * 1024
        ),
    )(
        tokens_in,
        norm_gain.reshape(1, D),
        query_weight,
        key_weight.T,
        value_weight.T,
        pool_weight,
        sink_logit.reshape(1, 2),
        pool_gain.reshape(1, 128),
        attention_out_weight,
        pool_out_weight,
    )


def solution(mesh):
    in_specs = (
        P(("sp", "tp"), None),
        P(),
        P("sp", "tp"),
        P("sp", "tp"),
        P("sp", "tp"),
        P("sp", "tp"),
        P("tp"),
        P("tp"),
        P("tp", "sp"),
        P("tp", "sp"),
    )
    out_specs = P(("sp", "tp"), None)
    return jax.shard_map(local, mesh=mesh, in_specs=in_specs, out_specs=out_specs, check_vma=False)
```

time: 57.4 us -> 48.5 us (0.84)
  the two profiles are of different devices: /device:TPU:1 before, /device:TPU:8 now
where the time goes in v3:
time: 48.5 us; the launch traced here: 48.3 us
  Pallas kernels  46.5 us (96%)
  local copies, waits for them, and re-layouts  1.77 us (4%)
    pallas_call x1, Pallas kernels, local(): pl.pallas_call(kernel, out_shape=jax.ShapeDtypeStruct((BLOCK, D), BF16),...  46.5 us
    unnamed x1, local copies, waits for them, and re-layouts  1.77 us

profile of v3, /device:TPU:8, one launch (start us, length us, event | category | flops | bytes accessed | tf_op | source)
XLA Modules:
  0.0 48.3 jit_solution(11366992163444854744)
XLA Ops:
  0.0 46.5 %shard_map.100 = bf16[96,2048]{1,0:T(8,128)(2,1)} custom-call(bf16[96,2048]{1,0:T(8,128)(2,1)} %x_hbm.1, f32[1,2048]{1,0:T(1,128)} %bitcast.7, bf16[128,128]{1,0:T(8,128)(2,1)} %wq_hbm.1, bf16[64,128]{1,0:T(8,128)(2,1)} %bitcast.5, bf16[64,128]{1,0:T(8,128)(2,1)} %bitcast.6, bf16[128,128]{1,0:T(8,128)(2,1)} %wp_hbm.1, f32[1,2]{1,0:T(1,128)} %bitcast.8, ...), custom_call_target="tpu_custom_call" | custom-call | tf_op jit(solution)/shard_map/pallas_call | solution.py:613
  46.5 1.8 %copy.12 = bf16[96,2048]{1,0:T(8,128)(2,1)} copy(bf16[96,2048]{1,0:T(8,128)(2,1)} %shard_map.100) | data formatting | bytes 786432

commit v4 on v3

--- a/solution.py
+++ b/solution.py
@@ -21,7 +21,9 @@
 CHUNK = 2 * BLOCK
 DEPTH = D // PLANE
 IN_COLS = 384
-N_GROUPS = 40
+N_GROUPS = 48
+PART = 16
+EARLY = 2
 
 
 class Groups:
@@ -84,7 +86,7 @@
     pgain_hbm,
     wa_hbm,
     wo_hbm,
-    out_ref,
+    out_hbm,
     xin,
     gain,
     pgain,
@@ -107,19 +109,20 @@
     cols_y,
     cols_core,
     cols_other,
-    cols_sp,
+    cols_chip,
+    cols_row,
+    cols_x,
+    cols_z,
+    terms,
     amine,
     apart,
-    far,
-    nbn,
-    nbp,
-    accn,
-    accp,
-    rfn,
-    rfp,
-    rn,
-    rp,
+    exact,
+    rounded,
+    from_prev,
+    from_next,
+    result,
     local_sems,
+    out_sems,
     send_sems,
     recv_sems,
 ):
@@ -214,9 +217,20 @@
 
     d_p, d_n, d_f = across(yp), across(yn), across(yf)
     c_core = one(cols_core, cols_other, partner, cols_other)
-    c_sp = groups.new(cols_sp.at[pl.ds(0, PLANE - 1)])
-    for step in range(1, PLANE):
-        c_sp.add(cols_sp.at[sp], cols_sp.at[sp], (lax.rem(sp + step, PLANE), tp))
+    c_x, c_z = groups.new(cols_x), groups.new(cols_z)
+    for n, by in enumerate((1, -1, 2)):
+        c_x.add(cols_chip, cols_x.at[n], (z * SIDE + turn(x, by), tp))
+        c_z.add(cols_row, cols_z.at[n], (turn(z, by) * SIDE + x, tp))
+    prefix_groups = (c_x, c_z)
+
+    def summed(own, slots, here=None):
+        total = own
+        for n, by in enumerate((-1, 1, 2)):
+            if here is None:
+                total = total + slots[n]
+            else:
+                total = total + jnp.where(turn(here, by) < here, slots[n], 0.0)
+        return total
 
     class Gather:
         def __init__(self, piece, sub, whole, direct, crossing_direct, shared=None):
@@ -339,17 +353,17 @@
     ins.near()
     ins.distant()
     c_y.arrived()
-    own_parity = columns + cols_y[0] + cols_y[1] + cols_y[2]
+    own_parity = summed(columns, cols_y)
     cols_core[...] = own_parity
     c_core.start()
     outs.near()
     ins.pass_on(0)
     c_core.arrived()
-    cols_sp[sp] = own_parity + cols_other[...]
+    cols_chip[...] = own_parity + cols_other[...]
 
     @pl.when(y == SIDE - 1)
     def _():
-        c_sp.start()
+        c_x.start()
 
     t_n0.arrived()
     f_n.start()
@@ -362,12 +376,20 @@
     ins.pass_on(1)
     ins.pass_on(2)
     outs.distant()
+
     t_n1.arrived()
     d_p.start(1)
     t_p0.arrived()
     d_n.start(0)
     outs.pass_on(-1)
     outs.pass_on(1)
+
+    @pl.when(y == SIDE - 1)
+    def _():
+        c_x.arrived()
+        cols_row[...] = summed(cols_chip[...], cols_x)
+        c_z.start()
+
     ins.finish()
 
     def spread(kv, rows, at):
@@ -405,27 +427,32 @@
     f_p.arrived()
     d_f.start(1)
     d_own.arrived()
-    project(y)
     d_p.arrived()
-    project(yp)
     d_n.arrived()
-    project(yn)
+    project(jnp.where(y == 0, yp, jnp.where(y == 3, y, yn)))
+    project(jnp.where(y == 3, yp, y))
+    project(jnp.where((y == 0) | (y == 3), yn, yp))
     outs.pass_on(2)
-    d_f.arrived()
-    project(yf)
-    outs.finish()
 
     @pl.when(y == SIDE - 1)
     def _():
-        c_sp.arrived()
-        earlier = lax.broadcasted_iota(jnp.int32, (PLANE, 1, D), 0) < sp
-        ahead = jnp.sum(jnp.where(earlier, cols_sp[...], 0.0), axis=0)
+        c_z.arrived()
+        nothing = jnp.zeros((1, D), F32)
+        ahead = summed(nothing, cols_z, z) + summed(nothing, cols_x, x)
         high = ahead.astype(BF16).astype(F32)
         middle = (ahead - high).astype(BF16).astype(F32)
         low = ahead - high - middle
         term = lax.broadcasted_iota(jnp.int32, (16, D), 0)
-        terms = jnp.where(term == 0, high, jnp.where(term == 1, middle, jnp.where(term == 2, low, 0.0)))
-        got = jnp.dot(terms.astype(BF16), win[:, 256:], preferred_element_type=F32)
+        rest = jnp.where(term == 1, middle, jnp.where(term == 2, low, 0.0))
+        terms[...] = jnp.where(term == 0, high, rest).astype(BF16)
+
+    d_f.arrived()
+    project(yf)
+    outs.finish()
+
+    @pl.when(y == SIDE - 1)
+    def _():
+        got = jnp.dot(terms[...], win[:, 256:], preferred_element_type=F32)
         before[...] = jnp.sum(got, axis=0, keepdims=True)
 
     span = WINDOW + BLOCK
@@ -482,83 +509,119 @@
         swap.start()
         return swap
 
-    def product(yy, put):
+    def product(yy, slot):
         mine = amine[rows_of((yy * 2 + c) * BLOCK, BLOCK), :]
         theirs = apart[rows_of(yy * BLOCK, BLOCK), :]
         for n in range(0, D, 512):
             cols = pl.ds(n, 512)
             got = jnp.dot(mine, wout[pl.ds(0, 256), cols], preferred_element_type=F32)
             got = got + jnp.dot(theirs, wout[pl.ds(256, 256), cols], preferred_element_type=F32)
-            put(cols, got)
-
-    top, bottom = pl.ds(0, HALF), pl.ds(HALF, HALF)
-    r_fn = one(far.at[top], rfn, up, rfn)
-    r_fp = one(far.at[bottom], rfp, down, rfp)
-    r_n1 = one(nbn.at[bottom], rn.at[bottom], up, rn.at[bottom])
-    r_p0 = one(nbp.at[top], rp.at[top], down, rp.at[top])
-    r_n0 = one(nbn.at[top], rn.at[top], up, rn.at[top])
-    r_p1 = one(nbp.at[bottom], rp.at[bottom], down, rp.at[bottom])
-
-    def put_far(cols, got):
-        far[:, cols] = got.astype(BF16)
-
-    def put_next(cols, got):
-        nbn[bottom, cols] = got[HALF:].astype(BF16)
-        accn[:, cols] = got[:HALF]
-
-    def put_prev(cols, got):
-        nbp[top, cols] = got[:HALF].astype(BF16)
-        accp[:, cols] = got[HALF:]
-
-    swap_f = first_half(yf)
-    attend(yf, c)
-    swap_n = first_half(yn)
+            exact[slot, :, cols] = got
+            if slot < 3:
+                rounded[slot, :, cols] = got.astype(BF16)
+
+    late = y == 2
+    order = [jnp.where(late, u, v) for u, v in ((yn, yf), (yp, yn), (yf, yp))]
+    at_far, at_next, at_prev = [jnp.where(late, u, v) for u, v in ((2, 0), (0, 1), (1, 2))]
+    lower = [pl.ds(n * PART, PART) for n in range(HALF // PART)]
+    upper = [pl.ds(HALF + n * PART, PART) for n in range(HALF // PART)]
+    r_fn = [one(rounded.at[at_far, p], from_prev.at[1, p], up, from_prev.at[1, p]) for p in lower]
+    r_fp = [one(rounded.at[at_far, p], from_next.at[1, p], down, from_next.at[1, p]) for p in upper]
+    r_n1 = groups.new(from_prev.at[0, pl.ds(HALF, HALF)])
+    r_p0 = groups.new(from_next.at[0, pl.ds(0, HALF)])
+    for p, q in zip(lower, upper):
+        r_n1.add(rounded.at[at_next, q], from_prev.at[0, q], up)
+        r_p0.add(rounded.at[at_prev, p], from_next.at[0, p], down)
+    r_n0 = [one(rounded.at[at_next, p], from_prev.at[0, p], up, from_prev.at[0, p]) for p in lower]
+    r_p1 = [one(rounded.at[at_prev, p], from_next.at[0, p], down, from_next.at[0, p]) for p in upper]
+    parts = range(len(lower))
+
+    def send_far():
+        for n in parts:
+            r_fn[n].start()
+            r_fp[n].start()
+
+    swap_a = first_half(order[0])
+    attend(order[0], c)
+    swap_b = first_half(order[1])
     outs.shares.arrived()
-    swap_f.arrived()
-    product(yf, put_far)
-    r_fn.start()
-    r_fp.start()
-    attend(yn, c)
-    swap_p = first_half(yp)
-    swap_n.arrived()
-    product(yn, put_next)
-    r_n1.start()
-    attend(yp, c)
-    swap_o = first_half(y)
-    swap_p.arrived()
-    product(yp, put_prev)
-    r_p0.start()
+    swap_a.arrived()
+    product(order[0], 0)
+
+    @pl.when(late)
+    def _():
+        r_n1.start(*parts[:EARLY])
+
+    @pl.when(y != 2)
+    def _():
+        send_far()
+
+    attend(order[1], c)
+    swap_b.arrived()
+    product(order[1], 1)
+
+    @pl.when(late)
+    def _():
+        r_p0.start(*parts[:EARLY])
+
+    @pl.when(y != 2)
+    def _():
+        r_n1.start()
+
+    swap_c = first_half(order[2])
+    attend(order[2], c)
+    swap_d = first_half(y)
+    swap_c.arrived()
+    product(order[2], 2)
+
+    @pl.when(late)
+    def _():
+        send_far()
+        if EARLY < len(parts):
+            r_n1.start(*parts[EARLY:])
+            r_p0.start(*parts[EARLY:])
+
+    @pl.when(y != 2)
+    def _():
+        r_p0.start()
+
     attend(y, c)
-    r_fn.arrived()
-    nbn[top, :] = (accn[...] + rfn[...].astype(F32)).astype(BF16)
-    r_n0.start()
-    r_fp.arrived()
-    nbp[bottom, :] = (accp[...] + rfp[...].astype(F32)).astype(BF16)
-    r_p1.start()
-    swap_o.arrived()
-
-    def put_own(cols, got):
-        accn[:, cols] = got[:HALF]
-        accp[:, cols] = got[HALF:]
-
-    product(y, put_own)
+    for n in parts:
+        r_fn[n].arrived()
+        rounded[at_next, lower[n], :] = (
+            exact[at_next, lower[n], :] + from_prev[1, lower[n], :].astype(F32)
+        ).astype(BF16)
+        r_n0[n].start()
+        r_fp[n].arrived()
+        rounded[at_prev, upper[n], :] = (
+            exact[at_prev, upper[n], :] + from_next[1, upper[n], :].astype(F32)
+        ).astype(BF16)
+        r_p1[n].start()
+
+    swap_d.arrived()
+    product(y, 3)
     r_n1.arrived()
-    accp[...] = accp[...] + rn[bottom, :].astype(F32)
+    for p in upper:
+        exact[3, p, :] = exact[3, p, :] + from_prev[0, p, :].astype(F32)
     r_p0.arrived()
-    accn[...] = accn[...] + rp[top, :].astype(F32)
-    r_n0.arrived()
-    out_ref[top, :] = (accn[...] + rn[top, :].astype(F32)).astype(BF16)
-    r_p1.arrived()
-    out_ref[bottom, :] = (accp[...] + rp[bottom, :].astype(F32)).astype(BF16)
+    for p in lower:
+        exact[3, p, :] = exact[3, p, :] + from_next[0, p, :].astype(F32)
+    for n in parts:
+        for group, p, got in ((r_n0[n], lower[n], from_prev), (r_p1[n], upper[n], from_next)):
+            group.arrived()
+            result[p, :] = (exact[3, p, :] + got[0, p, :].astype(F32)).astype(BF16)
+            pltpu.make_async_copy(result.at[p], out_hbm.at[p], out_sems.at[0]).start()
+    pltpu.make_async_copy(result, out_hbm, out_sems.at[0]).wait()
     for group in groups.made:
-        if group is not c_sp:
+        if group not in prefix_groups:
             group.sent()
 
     @pl.when(y == SIDE - 1)
     def _():
-        c_sp.sent()
-
-    assert len(groups.made) <= N_GROUPS
+        for group in prefix_groups:
+            group.sent()
+
+    assert len(groups.made) == N_GROUPS, len(groups.made)
 
 
 def local(
@@ -597,27 +660,28 @@
         ((3, 1, D), F32),
         ((1, D), F32),
         ((1, D), F32),
-        ((PLANE, 1, D), F32),
+        ((1, D), F32),
+        ((1, D), F32),
+        ((3, 1, D), F32),
+        ((3, 1, D), F32),
+        ((16, D), BF16),
         ((ROWS, 256), BF16),
         ((SIDE * BLOCK, 256), BF16),
-        ((BLOCK, D), BF16),
-        ((BLOCK, D), BF16),
-        ((BLOCK, D), BF16),
-        ((HALF, D), F32),
-        ((HALF, D), F32),
-        ((HALF, D), BF16),
-        ((HALF, D), BF16),
-        ((BLOCK, D), BF16),
+        ((4, BLOCK, D), F32),
+        ((3, BLOCK, D), BF16),
+        ((2, BLOCK, D), BF16),
+        ((2, BLOCK, D), BF16),
         ((BLOCK, D), BF16),
     ]
     return pl.pallas_call(
         kernel,
         out_shape=jax.ShapeDtypeStruct((BLOCK, D), BF16),
         in_specs=[hbm] * 10,
-        out_specs=pl.BlockSpec(memory_space=pltpu.VMEM),
+        out_specs=pl.BlockSpec(memory_space=pl.ANY),
         scratch_shapes=[pltpu.VMEM(shape, kind) for shape, kind in scratch]
         + [
             pltpu.SemaphoreType.DMA((7,)),
+            pltpu.SemaphoreType.DMA((1,)),
             pltpu.SemaphoreType.DMA((N_GROUPS,)),
             pltpu.SemaphoreType.DMA((N_GROUPS,)),
         ],

time: 48.5 us -> 46.5 us (0.959)
  the two profiles are of different devices: /device:TPU:8 before, /device:TPU:0 now
where the time goes in v4:
time: 46.5 us; the launch traced here: 46.3 us
  Pallas kernels  44.5 us (96%)
  local copies, waits for them, and re-layouts  1.77 us (4%)
    pallas_call x1, Pallas kernels, local(): pl.pallas_call(kernel, out_shape=jax.ShapeDtypeStruct((BLOCK, D), BF16),...  44.5 us
    unnamed x1, local copies, waits for them, and re-layouts  1.77 us

profile of v4, /device:TPU:0, one launch (start us, length us, event | category | flops | bytes accessed | tf_op | source)
XLA Modules:
  0.0 46.3 jit_solution(17234174885723672186)
XLA Ops:
  0.0 44.5 %shard_map.100 = bf16[96,2048]{1,0:T(8,128)(2,1)} custom-call(bf16[96,2048]{1,0:T(8,128)(2,1)} %x_hbm.1, f32[1,2048]{1,0:T(1,128)} %bitcast.7, bf16[128,128]{1,0:T(8,128)(2,1)} %wq_hbm.1, bf16[64,128]{1,0:T(8,128)(2,1)} %bitcast.5, bf16[64,128]{1,0:T(8,128)(2,1)} %bitcast.6, bf16[128,128]{1,0:T(8,128)(2,1)} %wp_hbm.1, f32[1,2]{1,0:T(1,128)} %bitcast.8, ...), custom_call_target="tpu_custom_call" | custom-call | tf_op jit(solution)/shard_map/pallas_call | solution.py:676
  44.5 1.8 %copy.12 = bf16[96,2048]{1,0:T(8,128)(2,1)} copy(bf16[96,2048]{1,0:T(8,128)(2,1)} %shard_map.100) | data formatting | bytes 786432

commit v5 on v4

--- a/solution.py
+++ b/solution.py
@@ -1,3 +1,5 @@
+import math
+
 import jax
 import jax.numpy as jnp
 from jax import lax
@@ -22,23 +24,37 @@
 DEPTH = D // PLANE
 IN_COLS = 384
 N_GROUPS = 48
+SEND_SEMS = 4
+SENT_ROWS = 12800
 PART = 16
 EARLY = 2
 
 
 class Groups:
     def __init__(self, send_sems, recv_sems):
-        self.send_sems, self.recv_sems, self.made = send_sems, recv_sems, []
-
-    def new(self, whole):
-        group = Group(self.send_sems.at[len(self.made)], self.recv_sems.at[len(self.made)], whole)
+        self.send_sems, self.recv_sems, self.made, self.lone = send_sems, recv_sems, [], []
+
+    def new(self, whole, lone=False):
+        number = len(self.made)
+        place = SEND_SEMS + len(self.lone) if lone else number % SEND_SEMS
+        group = Group(self.send_sems.at[place], self.recv_sems.at[number], whole)
         self.made.append(group)
+        if lone:
+            self.lone.append(group)
         return group
 
     def one(self, src, dst, device, land):
         group = self.new(land)
         group.add(src, dst, device)
         return group
+
+    def all_sent(self, rows):
+        for n in range(SEND_SEMS):
+            here = [g for g in self.made[n::SEND_SEMS] if g not in self.lone]
+            size = sum(math.prod(g.whole.shape) * g.whole.dtype.itemsize for g in here)
+            assert size % 4096 == 0 and size <= SENT_ROWS * 256, size
+            part = rows.at[pl.ds(0, size // 256)]
+            here[0].copy(part, part, here[0].device).wait_send()
 
 
 class Group:
@@ -86,7 +102,8 @@
     pgain_hbm,
     wa_hbm,
     wo_hbm,
-    out_hbm,
+    own_hbm,
+    last_hbm,
     xin,
     gain,
     pgain,
@@ -118,9 +135,10 @@
     apart,
     exact,
     rounded,
-    from_prev,
-    from_next,
-    result,
+    far_prev,
+    far_next,
+    near,
+    sent,
     local_sems,
     out_sems,
     send_sems,
@@ -217,11 +235,10 @@
 
     d_p, d_n, d_f = across(yp), across(yn), across(yf)
     c_core = one(cols_core, cols_other, partner, cols_other)
-    c_x, c_z = groups.new(cols_x), groups.new(cols_z)
+    c_x, c_z = groups.new(cols_x, True), groups.new(cols_z, True)
     for n, by in enumerate((1, -1, 2)):
         c_x.add(cols_chip, cols_x.at[n], (z * SIDE + turn(x, by), tp))
         c_z.add(cols_row, cols_z.at[n], (turn(z, by) * SIDE + x, tp))
-    prefix_groups = (c_x, c_z)
 
     def summed(own, slots, here=None):
         total = own
@@ -346,8 +363,8 @@
     for group in (c_y, t_n0, t_p1, t_n1, t_p0):
         group.start()
     ins.begin()
+    ins.cross(0)
     outs.begin()
-    ins.cross(0)
     outs.cross(0)
     d_own.start()
     ins.near()
@@ -525,15 +542,15 @@
     at_far, at_next, at_prev = [jnp.where(late, u, v) for u, v in ((2, 0), (0, 1), (1, 2))]
     lower = [pl.ds(n * PART, PART) for n in range(HALF // PART)]
     upper = [pl.ds(HALF + n * PART, PART) for n in range(HALF // PART)]
-    r_fn = [one(rounded.at[at_far, p], from_prev.at[1, p], up, from_prev.at[1, p]) for p in lower]
-    r_fp = [one(rounded.at[at_far, p], from_next.at[1, p], down, from_next.at[1, p]) for p in upper]
-    r_n1 = groups.new(from_prev.at[0, pl.ds(HALF, HALF)])
-    r_p0 = groups.new(from_next.at[0, pl.ds(0, HALF)])
+    r_fn = [one(rounded.at[at_far, p], far_prev.at[p], up, far_prev.at[p]) for p in lower]
+    r_fp = [one(rounded.at[at_far, p], far_next.at[p], down, far_next.at[p]) for p in upper]
+    r_n1 = groups.new(near.at[pl.ds(HALF, HALF)])
+    r_p0 = groups.new(near.at[pl.ds(0, HALF)])
     for p, q in zip(lower, upper):
-        r_n1.add(rounded.at[at_next, q], from_prev.at[0, q], up)
-        r_p0.add(rounded.at[at_prev, p], from_next.at[0, p], down)
-    r_n0 = [one(rounded.at[at_next, p], from_prev.at[0, p], up, from_prev.at[0, p]) for p in lower]
-    r_p1 = [one(rounded.at[at_prev, p], from_next.at[0, p], down, from_next.at[0, p]) for p in upper]
+        r_n1.add(rounded.at[at_next, q], near.at[q], up)
+        r_p0.add(rounded.at[at_prev, p], near.at[p], down)
+    r_n0 = [one(rounded.at[at_next, p], last_hbm.at[p], up, last_hbm.at[p]) for p in lower]
+    r_p1 = [one(rounded.at[at_prev, p], last_hbm.at[p], down, last_hbm.at[p]) for p in upper]
     parts = range(len(lower))
 
     def send_far():
@@ -589,37 +606,33 @@
     for n in parts:
         r_fn[n].arrived()
         rounded[at_next, lower[n], :] = (
-            exact[at_next, lower[n], :] + from_prev[1, lower[n], :].astype(F32)
+            exact[at_next, lower[n], :] + far_prev[lower[n], :].astype(F32)
         ).astype(BF16)
         r_n0[n].start()
         r_fp[n].arrived()
         rounded[at_prev, upper[n], :] = (
-            exact[at_prev, upper[n], :] + from_next[1, upper[n], :].astype(F32)
+            exact[at_prev, upper[n], :] + far_next[upper[n], :].astype(F32)
         ).astype(BF16)
         r_p1[n].start()
 
     swap_d.arrived()
     product(y, 3)
     r_n1.arrived()
-    for p in upper:
-        exact[3, p, :] = exact[3, p, :] + from_prev[0, p, :].astype(F32)
     r_p0.arrived()
-    for p in lower:
-        exact[3, p, :] = exact[3, p, :] + from_next[0, p, :].astype(F32)
+    for p in lower + upper:
+        exact[3, p, :] = exact[3, p, :] + near[p, :].astype(F32)
+    mine = pltpu.make_async_copy(exact.at[3], own_hbm, out_sems.at[0])
+    mine.start()
     for n in parts:
-        for group, p, got in ((r_n0[n], lower[n], from_prev), (r_p1[n], upper[n], from_next)):
-            group.arrived()
-            result[p, :] = (exact[3, p, :] + got[0, p, :].astype(F32)).astype(BF16)
-            pltpu.make_async_copy(result.at[p], out_hbm.at[p], out_sems.at[0]).start()
-    pltpu.make_async_copy(result, out_hbm, out_sems.at[0]).wait()
-    for group in groups.made:
-        if group not in prefix_groups:
-            group.sent()
+        r_n0[n].arrived()
+        r_p1[n].arrived()
+    mine.wait()
+    groups.all_sent(sent)
 
     @pl.when(y == SIDE - 1)
     def _():
-        for group in prefix_groups:
-            group.sent()
+        c_x.sent()
+        c_z.sent()
 
     assert len(groups.made) == N_GROUPS, len(groups.made)
 
@@ -669,20 +682,24 @@
         ((SIDE * BLOCK, 256), BF16),
         ((4, BLOCK, D), F32),
         ((3, BLOCK, D), BF16),
-        ((2, BLOCK, D), BF16),
-        ((2, BLOCK, D), BF16),
         ((BLOCK, D), BF16),
+        ((BLOCK, D), BF16),
+        ((BLOCK, D), BF16),
+        ((SENT_ROWS, 128), BF16),
     ]
-    return pl.pallas_call(
+    own, last = pl.pallas_call(
         kernel,
-        out_shape=jax.ShapeDtypeStruct((BLOCK, D), BF16),
+        out_shape=[
+            jax.ShapeDtypeStruct((BLOCK, D), F32),
+            jax.ShapeDtypeStruct((BLOCK, D), BF16),
+        ],
         in_specs=[hbm] * 10,
-        out_specs=pl.BlockSpec(memory_space=pl.ANY),
+        out_specs=[pl.BlockSpec(memory_space=pl.ANY)] * 2,
         scratch_shapes=[pltpu.VMEM(shape, kind) for shape, kind in scratch]
         + [
             pltpu.SemaphoreType.DMA((7,)),
             pltpu.SemaphoreType.DMA((1,)),
-            pltpu.SemaphoreType.DMA((N_GROUPS,)),
+            pltpu.SemaphoreType.DMA((SEND_SEMS + 2,)),
             pltpu.SemaphoreType.DMA((N_GROUPS,)),
         ],
         compiler_params=pltpu.CompilerParams(
@@ -700,6 +717,7 @@
         attention_out_weight,
         pool_out_weight,
     )
+    return (own + last.astype(F32)).astype(BF16)
 
 
 def solution(mesh):

time: 46.5 us -> 45.7 us (0.983)
  other arithmetic: 0 us -> 2.06 us
  local copies, waits for them, and re-layouts: 1.77 us -> 0 us
  Pallas kernels: 44.5 us -> 43.5 us
    convert_element_type x0 -> x1, other arithmetic: none -> 2.06 us  [local(): return (own + last.astype(F32)).astype(BF16)]
    unnamed x1 -> x0, local copies, waits for them, and re-layouts: 1.77 us -> none
    pallas_call x1, Pallas kernels: 44.5 us -> 43.5 us  [local(): pl.pallas_call(kernel, out_shape=[jax.ShapeDtypeStruct((BLOCK, D), F32),...]
where the time goes in v5:
time: 45.7 us; the launch traced here: 45.6 us
  Pallas kernels  43.5 us (95%)
  other arithmetic  2.06 us (5%)
    pallas_call x1, Pallas kernels, local(): pl.pallas_call(kernel, out_shape=[jax.ShapeDtypeStruct((BLOCK, D), F32),...  43.5 us
    convert_element_type x1, other arithmetic, local(): return (own + last.astype(F32)).astype(BF16)  2.06 us

profile of v5, /device:TPU:0, one launch (start us, length us, event | category | flops | bytes accessed | tf_op | source)
XLA Modules:
  0.0 45.6 jit_solution(3856470337784270957)
XLA Ops:
  0.0 43.5 %shard_map.100 = (f32[96,2048]{1,0:T(8,128)}, bf16[96,2048]{1,0:T(8,128)(2,1)}) custom-call(bf16[96,2048]{1,0:T(8,128)(2,1)} %x_hbm.1, f32[1,2048]{1,0:T(1,128)} %bitcast.7, bf16[128,128]{1,0:T(8,128)(2,1)} %wq_hbm.1, bf16[64,128]{1,0:T(8,128)(2,1)} %bitcast.5, bf16[64,128]{1,0:T(8,128)(2,1)} %bitcast.6, bf16[128,128]{1,0:T(8,128)(2,1)} %wp_hbm.1, ...), custom_call_target="tpu_custom_call" | custom-call | tf_op jit(solution)/shard_map/pallas_call | solution.py:690
  43.5 2.1 %add_convert_fusion = bf16[96,2048]{1,0:T(8,128)(2,1)} fusion(f32[96,2048]{1,0:T(8,128)} %get-tuple-element.7, bf16[96,2048]{1,0:T(8,128)(2,1)} %get-tuple-element.8), kind=kLoop, calls=%fused_computation | loop fusion | flops 589824 | bytes 1572864 | tf_op jit(solution)/shard_map/convert_element_type | solution.py:720

commit v6 on v5

--- a/solution.py
+++ b/solution.py
@@ -138,6 +138,7 @@
     far_prev,
     far_next,
     near,
+    result,
     sent,
     local_sems,
     out_sems,
@@ -449,7 +450,6 @@
     project(jnp.where(y == 0, yp, jnp.where(y == 3, y, yn)))
     project(jnp.where(y == 3, yp, y))
     project(jnp.where((y == 0) | (y == 3), yn, yp))
-    outs.pass_on(2)
 
     @pl.when(y == SIDE - 1)
     def _():
@@ -465,6 +465,7 @@
 
     d_f.arrived()
     project(yf)
+    outs.pass_on(2)
     outs.finish()
 
     @pl.when(y == SIDE - 1)
@@ -620,8 +621,8 @@
     r_n1.arrived()
     r_p0.arrived()
     for p in lower + upper:
-        exact[3, p, :] = exact[3, p, :] + near[p, :].astype(F32)
-    mine = pltpu.make_async_copy(exact.at[3], own_hbm, out_sems.at[0])
+        result[p, :] = (exact[3, p, :] + near[p, :].astype(F32)).astype(BF16)
+    mine = pltpu.make_async_copy(result, own_hbm, out_sems.at[0])
     mine.start()
     for n in parts:
         r_n0[n].arrived()
@@ -685,12 +686,13 @@
         ((BLOCK, D), BF16),
         ((BLOCK, D), BF16),
         ((BLOCK, D), BF16),
+        ((BLOCK, D), BF16),
         ((SENT_ROWS, 128), BF16),
     ]
     own, last = pl.pallas_call(
         kernel,
         out_shape=[
-            jax.ShapeDtypeStruct((BLOCK, D), F32),
+            jax.ShapeDtypeStruct((BLOCK, D), BF16),
             jax.ShapeDtypeStruct((BLOCK, D), BF16),
         ],
         in_specs=[hbm] * 10,
@@ -717,7 +719,7 @@
         attention_out_weight,
         pool_out_weight,
     )
-    return (own + last.astype(F32)).astype(BF16)
+    return (own.astype(F32) + last.astype(F32)).astype(BF16)
 
 
 def solution(mesh):

time: 45.7 us -> 45.6 us (level)
  no operation moved by 1% of the time
where the time goes in v6:
time: 45.6 us; the launch traced here: 45.5 us
  Pallas kernels  43.5 us (95%)
  other arithmetic  1.96 us (4%)
    pallas_call x1, Pallas kernels, local(): pl.pallas_call(kernel, out_shape=[jax.ShapeDtypeStruct((BLOCK, D), BF16),...  43.5 us
    convert_element_type x1, other arithmetic, local(): return (own.astype(F32) + last.astype(F32)).astype(BF16)  1.96 us

profile of v6, /device:TPU:0, one launch (start us, length us, event | category | flops | bytes accessed | tf_op | source)
XLA Modules:
  0.0 45.5 jit_solution(18295533636011736515)
XLA Ops:
  0.0 43.5 %shard_map.100 = (bf16[96,2048]{1,0:T(8,128)(2,1)}, bf16[96,2048]{1,0:T(8,128)(2,1)}) custom-call(bf16[96,2048]{1,0:T(8,128)(2,1)} %x_hbm.1, f32[1,2048]{1,0:T(1,128)} %bitcast.7, bf16[128,128]{1,0:T(8,128)(2,1)} %wq_hbm.1, bf16[64,128]{1,0:T(8,128)(2,1)} %bitcast.5, bf16[64,128]{1,0:T(8,128)(2,1)} %bitcast.6, bf16[128,128]{1,0:T(8,128)(2,1)} %wp_hbm.1, ...), custom_call_target="tpu_custom_call" | custom-call | tf_op jit(solution)/shard_map/pallas_call | solution.py:692
  43.5 2.0 %add_convert_fusion = bf16[96,2048]{1,0:T(8,128)(2,1)} fusion(bf16[96,2048]{1,0:T(8,128)(2,1)} %get-tuple-element.8, bf16[96,2048]{1,0:T(8,128)(2,1)} %get-tuple-element.7), kind=kLoop, calls=%fused_computation | loop fusion | flops 786432 | bytes 1179648 | tf_op jit(solution)/shard_map/convert_element_type | solution.py:722

commit v7 on v6

--- a/solution.py
+++ b/solution.py
@@ -27,7 +27,7 @@
 SEND_SEMS = 4
 SENT_ROWS = 12800
 PART = 16
-EARLY = 2
+EARLY = 1
 
 
 class Groups:

time: 45.6 us -> 46.3 us (1.015); the launches traced: 45.5 us -> 45.5 us
  no operation moved by 1% of the time
where the time goes in v7:
time: 46.3 us; the launch traced here: 45.5 us
  Pallas kernels  43.5 us (94%)
  other arithmetic  1.96 us (4%)
    pallas_call x1, Pallas kernels, local(): pl.pallas_call(kernel, out_shape=[jax.ShapeDtypeStruct((BLOCK, D), BF16),...  43.5 us
    convert_element_type x1, other arithmetic, local(): return (own.astype(F32) + last.astype(F32)).astype(BF16)  1.96 us

profile of v7, /device:TPU:0, one launch (start us, length us, event | category | flops | bytes accessed | tf_op | source)
XLA Modules:
  0.0 45.5 jit_solution(16060658111012398771)
XLA Ops:
  0.0 43.5 %shard_map.100 = (bf16[96,2048]{1,0:T(8,128)(2,1)}, bf16[96,2048]{1,0:T(8,128)(2,1)}) custom-call(bf16[96,2048]{1,0:T(8,128)(2,1)} %x_hbm.1, f32[1,2048]{1,0:T(1,128)} %bitcast.7, bf16[128,128]{1,0:T(8,128)(2,1)} %wq_hbm.1, bf16[64,128]{1,0:T(8,128)(2,1)} %bitcast.5, bf16[64,128]{1,0:T(8,128)(2,1)} %bitcast.6, bf16[128,128]{1,0:T(8,128)(2,1)} %wp_hbm.1, ...), custom_call_target="tpu_custom_call" | custom-call | tf_op jit(solution)/shard_map/pallas_call | solution.py:692
  43.5 2.0 %add_convert_fusion = bf16[96,2048]{1,0:T(8,128)(2,1)} fusion(bf16[96,2048]{1,0:T(8,128)(2,1)} %get-tuple-element.8, bf16[96,2048]{1,0:T(8,128)(2,1)} %get-tuple-element.7), kind=kLoop, calls=%fused_computation | loop fusion | flops 786432 | bytes 1179648 | tf_op jit(solution)/shard_map/convert_element_type | solution.py:722
